TPU v7x, 512 devices: a whole 4x4x16 slice. The times are simulated.
512 devices in a mesh: sp: 64 (over z, y), tp: 8 (over x, core).
Axes of the slice: x: 4, y: 4, z: 16, core: 2. Of those that a mesh axis runs over, the one named last changes fastest.
Arguments:
- tokens: bfloat16 [4096, 1, 2048], P('sp'), may hold values from -6 to 6
- queries: bfloat16 [4096, 1, 1024], P('sp', None, 'tp'), may hold values from -15 to 15
- key_values: bfloat16 [4096, 1, 1024], P('sp', None, 'tp'), may hold values from -6 to 6
- stop_bias: bfloat16 [4096, 1, 16], P('sp', None, 'tp'), may hold values from -20 to 0
- out_proj: bfloat16 [1024, 2048], P('tp'), may hold values from -0.375 to 0.375
- norm_gain: float32 [2048], replicated, may hold values from 0.1 to 1.9
- up_proj: bfloat16 [2048, 4096], P('sp', 'tp'), may hold values from -0.125 to 0.125
- down_proj: bfloat16 [4096, 2048], P('tp', 'sp'), may hold values from -0.09375 to 0.09375
Outputs:
- layer_out: bfloat16 [4096, 1, 2048], P(('sp', 'tp'))
All inputs are finite; a program needn't handle non-finite values.
Results may differ from a plain program's by a relative error of at most 0.018.
Values may be sent and summed in bfloat16 or wider, within the bound.
A program may use at most 64 MiB of HBM per device.

v0:
```python
import math

import jax
import jax.numpy as jnp
from jax import lax
from jax.sharding import PartitionSpec as P

HEAD = 64


EPSILON = 1e-06


def side_by_side(arrays, axis, dim, along):
    widths = [a.shape[along] for a in arrays]
    both = jnp.concatenate(arrays, axis=along)
    out = lax.all_gather(both, axis, axis=dim, tiled=True)
    return tuple(jnp.split(out, [sum(widths[:k]) for k in range(1, len(widths))], axis=along))


def from_everyone(value, axis):
    copies = jnp.broadcast_to(value, (lax.axis_size(axis), *value.shape))
    return lax.all_to_all(copies, axis, split_axis=0, concat_axis=0, tiled=True)


def of_everyone(value, axis):
    everything = from_everyone(value, axis)
    return jnp.sum(everything.astype(jnp.float32), axis=0)


def in_blocks(value, dim, size):
    before, after = (value.shape[:dim], value.shape[dim + 1 :])
    return jnp.moveaxis(value.reshape(*before, size, -1, *after), dim, 0)


def summed_on_arrival(value, axis, dim):
    size = lax.axis_size(axis)
    pieces = lax.all_to_all(in_blocks(value, dim, size), axis, 0, 0, tiled=True)
    return jnp.sum(pieces.astype(jnp.float32), axis=0)


def rms_scale(residual, gain):
    values = residual.astype(jnp.float32)
    factor = lax.rsqrt(jnp.mean(values * values, axis=-1, keepdims=True) + EPSILON)
    return (values * factor * gain).astype(jnp.bfloat16)


def sweep_keys(totals, pieces, shard_rows, step_fn):
    kv_rows, bias_rows = pieces
    shards = kv_rows.shape[0] // shard_rows
    group_shards = math.gcd(shards, max(1, 1024 // shard_rows))
    span_rows = group_shards * shard_rows

    def advance(number, running):
        first_row = number * span_rows
        kv_block = lax.dynamic_slice_in_dim(kv_rows, first_row, span_rows, 0)
        bias_block = lax.dynamic_slice_in_dim(bias_rows, first_row, span_rows, 0)
        return step_fn(running, kv_block, bias_block, first_row, group_shards)

    return lax.fori_loop(0, shards // group_shards, advance, totals)


def body(tokens, queries, key_values, stop_bias, out_proj, norm_gain, up_proj, down_proj):
    row_count = tokens.shape[0]
    seq_count = tokens.shape[1]
    head_count = queries.shape[2] // HEAD
    kv_count = key_values.shape[2] // (2 * HEAD)
    group_size = head_count // kv_count
    n_shards = lax.axis_size("sp")
    query_start = lax.axis_index("sp") * row_count
    query_pos = query_start + lax.iota(jnp.int32, row_count)
    q_heads = queries.reshape(row_count, seq_count, kv_count, group_size, HEAD).transpose(
        1, 2, 3, 0, 4
    )
    q_heads = q_heads.reshape(seq_count, kv_count, group_size * row_count, HEAD)

    def stick_block(kv_block, bias_block, key_start):
        span_rows = kv_block.shape[0]
        key_pairs = kv_block.reshape(span_rows, seq_count, kv_count, 2 * HEAD)
        keys_part = key_pairs[..., :HEAD]
        values_part = key_pairs[..., HEAD:]
        scores = (
            jnp.einsum("bgmd,sbgd->bgms", q_heads, keys_part, preferred_element_type=jnp.float32)
            * 0.125
        )
        bias_float = jnp.transpose(bias_block, (1, 2, 0)).astype(jnp.float32)
        scores = (
            scores.reshape(seq_count, head_count, row_count, span_rows) + bias_float[:, :, None, :]
        )
        key_pos = key_start + lax.iota(jnp.int32, span_rows)
        strict = key_pos[None, :] < query_pos[:, None]
        log_pass = jnp.where(strict, jax.nn.log_sigmoid(-scores), 0.0)
        return (scores, strict, log_pass, values_part)

    def weigh(scores, strict, after_sum, values_part):
        span_rows = scores.shape[3]
        weights = jnp.where(strict, jnp.exp(jax.nn.log_sigmoid(scores) + after_sum), 0.0).astype(
            jnp.bfloat16
        )
        weights = weights.reshape(seq_count, kv_count, group_size * row_count, span_rows)
        return jnp.einsum(
            "bgms,sbgd->bgmd", weights, values_part, preferred_element_type=jnp.float32
        )

    empty_out = jnp.zeros((seq_count, kv_count, group_size * row_count, HEAD), jnp.float32)

    def sum_step(sums_table, kv_block, bias_block, key_start, shard_group):

        def sum_compute(table_in):
            scores, strict, log_pass, values_part = stick_block(kv_block, bias_block, key_start)
            block_sums = log_pass.reshape(
                seq_count, head_count, row_count, shard_group, row_count
            ).sum(axis=4)
            slot_index = key_start // row_count
            current = lax.dynamic_slice_in_dim(table_in, slot_index, shard_group, 0)
            return lax.dynamic_update_slice_in_dim(
                table_in, current + jnp.transpose(block_sums, (3, 0, 1, 2)), slot_index, 0
            )

        return lax.cond(
            key_start < query_start + row_count, sum_compute, lambda table_in: table_in, sums_table
        )

    empty_table = jnp.zeros((n_shards, seq_count, head_count, row_count), jnp.float32)
    sums_table = sweep_keys(
        empty_table, side_by_side((key_values, stop_bias), "sp", 0, 2), row_count, sum_step
    )
    offsets = lax.cumsum(sums_table, axis=0, reverse=True) - sums_table

    def out_step(outputs, kv_block, bias_block, key_start, shard_group):

        def out_compute(running):
            scores, strict, log_pass, values_part = stick_block(kv_block, bias_block, key_start)
            span_rows = kv_block.shape[0]
            split_pass = log_pass.reshape(seq_count, head_count, row_count, shard_group, row_count)
            within = lax.cumsum(split_pass, axis=4, reverse=True) - split_pass
            carried = lax.dynamic_slice_in_dim(offsets, key_start // row_count, shard_group, 0)
            carried = jnp.transpose(carried, (1, 2, 3, 0))[..., None]
            after_sum = (within + carried).reshape(seq_count, head_count, row_count, span_rows)
            return running + weigh(scores, strict, after_sum, values_part)

        return lax.cond(
            key_start < query_start + row_count, out_compute, lambda running: running, outputs
        )

    accum_out = sweep_keys(
        empty_out, side_by_side((key_values, stop_bias), "sp", 0, 2), row_count, out_step
    )
    attended = accum_out.reshape(seq_count, kv_count, group_size, row_count, HEAD).transpose(
        3, 0, 1, 2, 4
    )
    attended = attended.reshape(row_count * seq_count, head_count * HEAD).astype(jnp.bfloat16)
    share_tokens = row_count // lax.axis_size("tp")
    share_rows = share_tokens * seq_count
    tp_index = lax.axis_index("tp")
    projected = of_everyone(
        jnp.dot(attended, out_proj, preferred_element_type=jnp.float32).astype(jnp.bfloat16), "tp"
    ).astype(jnp.float32)
    flat_tokens = tokens.reshape(row_count * seq_count, tokens.shape[2])
    residual = (flat_tokens.astype(jnp.float32) + projected).astype(jnp.bfloat16)
    normed = rms_scale(residual, norm_gain)
    residual_share = lax.dynamic_slice_in_dim(residual, tp_index * share_rows, share_rows, 0)
    up_values = jnp.dot(
        normed,
        lax.all_gather(up_proj, "sp", axis=0, tiled=True),
        preferred_element_type=jnp.float32,
    )
    hidden = jnp.square(jax.nn.relu(up_values)).astype(jnp.bfloat16)
    partial_terms = jnp.dot(
        hidden,
        lax.all_gather(down_proj, "sp", axis=1, tiled=True),
        preferred_element_type=jnp.float32,
    )
    update = summed_on_arrival(partial_terms.astype(jnp.bfloat16), "tp", 0)
    result = (residual_share.astype(jnp.float32) + update).astype(jnp.bfloat16)
    return result.reshape(share_tokens, seq_count, result.shape[1])


def solution(mesh):
    return jax.shard_map(
        body,
        mesh=mesh,
        in_specs=(
            P("sp", None, None),
            P("sp", None, "tp"),
            P("sp", None, "tp"),
            P("sp", None, "tp"),
            P("tp", None),
            P(),
            P("sp", "tp"),
            P("tp", "sp"),
        ),
        out_specs=P(("sp", "tp"), None, None),
        check_vma=False,
    )
```

profile of v0, /device:TPU:480, one launch (start us, length us, event | category | flops | bytes accessed | tf_op | source)
XLA Modules:
  0.0 486.1 jit_solution(16853821687320576494)
XLA Ops:
  6.5 0.8 copy.44
  7.4 1.3 pad_maximum_fusion
  8.8 0.7 all-gather.6.cloned.1.call-update
  10.2 0.8 reshape.330
  11.0 137.0 %all-gather.4.cloned.1.call-done = bf16[4096,1,130]{2,0,1:T(8,128)(2,1)} async-done(((bf16[64,1,130]{2,0,1:T(8,128)(2,1)}), bf16[4096,1,130]{2,0,1:T(8,128)(2,1)}) %all-gather.4.cloned.1.call-update) | async-done | bytes 1064976 | tf_op jit(solution)/shard_map/all_gather | solution.py:17
  148.1 1.3 split.11
  149.8 2.3 split.10
  152.1 23.5 %while.38 = (s32[]{:T(128)}, f32[64,1,2,64]{3,2,1,0:T(2,128)S(1)}, s32[]{:T(128)}, bf16[4096,1,128]{2,0,1:T(8,128)(2,1)}, bf16[1,1,128,64]{3,2,1,0:T(8,128)(2,1)...) while((s32[]{:T(128)}, f32[64,1,2,64]{3,2,1,0:T(2,128)S(1)}, ...), condition=%wide.region_4.5_spmd.clone, body=%wide.region_0.4_spmd.clone.sunk | while | flops 18289752 | bytes 3118492 | solution.py:60
  152.1 5.8 %conditional.6 = (f32[64,1,2,64]{3,2,1,0:T(2,128)S(1)}) conditional(s32[]{:T(128)} %convert_element_type.148, f32[64,1,2,64]{3,2,1,0:T(2,128)S(1)} %get-tuple-element.781, (s32[]{:T(128)}, f32[64,1,2,64]{3,2,1,0:T(2,128)S(1)}, s32[]{:T(128)}, bf16[4096,1,128]{2,0,1:T(8,128)(2,1)}, bf16[1,1,128,64]{3,2,1,0:T(8,128)(2,1)S(1)}, ...), branch_computations={%region_1.0_spmd, %region_2.3_spmd} | conditional | flops 18289748 | bytes 3118061 | solution.py:120
  152.1 1.0 dynamic-slice_bitcast_fusion
  154.2 3.6 fusion.7
  158.0 5.8 %conditional.6 = (f32[64,1,2,64]{3,2,1,0:T(2,128)S(1)}) conditional(s32[]{:T(128)} %convert_element_type.148, f32[64,1,2,64]{3,2,1,0:T(2,128)S(1)} %get-tuple-element.781, (s32[]{:T(128)}, f32[64,1,2,64]{3,2,1,0:T(2,128)S(1)}, s32[]{:T(128)}, bf16[4096,1,128]{2,0,1:T(8,128)(2,1)}, bf16[1,1,128,64]{3,2,1,0:T(8,128)(2,1)S(1)}, ...), branch_computations={%region_1.0_spmd, %region_2.3_spmd} | conditional | flops 18289748 | bytes 3118061 | solution.py:120
  158.0 1.0 dynamic-slice_bitcast_fusion
  160.1 3.6 fusion.7
  163.9 5.8 %conditional.6 = (f32[64,1,2,64]{3,2,1,0:T(2,128)S(1)}) conditional(s32[]{:T(128)} %convert_element_type.148, f32[64,1,2,64]{3,2,1,0:T(2,128)S(1)} %get-tuple-element.781, (s32[]{:T(128)}, f32[64,1,2,64]{3,2,1,0:T(2,128)S(1)}, s32[]{:T(128)}, bf16[4096,1,128]{2,0,1:T(8,128)(2,1)}, bf16[1,1,128,64]{3,2,1,0:T(8,128)(2,1)S(1)}, ...), branch_computations={%region_1.0_spmd, %region_2.3_spmd} | conditional | flops 18289748 | bytes 3118061 | solution.py:120
  163.9 1.0 dynamic-slice_bitcast_fusion
  166.0 3.6 fusion.7
  169.8 5.8 %conditional.6 = (f32[64,1,2,64]{3,2,1,0:T(2,128)S(1)}) conditional(s32[]{:T(128)} %convert_element_type.148, f32[64,1,2,64]{3,2,1,0:T(2,128)S(1)} %get-tuple-element.781, (s32[]{:T(128)}, f32[64,1,2,64]{3,2,1,0:T(2,128)S(1)}, s32[]{:T(128)}, bf16[4096,1,128]{2,0,1:T(8,128)(2,1)}, bf16[1,1,128,64]{3,2,1,0:T(8,128)(2,1)S(1)}, ...), branch_computations={%region_1.0_spmd, %region_2.3_spmd} | conditional | flops 18289748 | bytes 3118061 | solution.py:120
  169.8 1.0 dynamic-slice_bitcast_fusion
  171.9 3.6 fusion.7
  176.5 253.4 %while.39 = (s32[]{:T(128)}, f32[1,1,128,64]{2,3,1,0:T(8,128)}, s32[]{:T(128)}, bf16[4096,1,128]{2,0,1:T(8,128)(2,1)}, bf16[1,1,128,64]{3,2,1,0:T(8,128)(2,1)S(1...) while((s32[]{:T(128)}, f32[1,1,128,64]{2,3,1,0:T(8,128)}, ...), condition=%wide.region_10.11_spmd.clone, body=%wide.region_6.10_spmd.clone.sunk | while | flops 46151768 | bytes 16168656 | solution.py:60
  176.5 63.3 %conditional.7 = (f32[1,1,128,64]{2,3,1,0:T(8,128)}) conditional(s32[]{:T(128)} %convert_element_type.149, f32[1,1,128,64]{2,3,1,0:T(8,128)} %get-tuple-element.809, (s32[]{:T(128)}, s32[]{:T(128)}, bf16[4096,1,128]{2,0,1:T(8,128)(2,1)}, bf16[1,1,128,64]{3,2,1,0:T(8,128)(2,1)S(1)}, bf16[4096,1,2]{0,2,1:T(2,128)(2,1)S(1)}, ...), branch_computations={%region_7.7_spmd, %region_8.9_spmd} | conditional | flops 46151764 | bytes 16168209 | solution.py:142
  176.8 1.4 add.310
  178.2 1.0 dynamic-slice_bitcast_fusion.1
  181.6 54.7 %reduce_window_sum.22 = f32[1,2,64,16,64]{4,3,2,1,0:T(8,128)S(1)} reduce-window(f32[1,2,64,16,64]{4,3,2,1,0:T(8,128)S(1)} %fusion.13, f32[]{:T(128)} %constant.213.clone), window={size=1x1x1x1x64 pad=0_0x0_0x0_0x0_0x0_63}, to_apply=%region_9.8 | reduce-window | flops 8257536 | bytes 1048580 | tf_op jit(solution)/shard_map/while/body/eval_jaxpr/cond/branch_1_fun/reduce_window_sum | solution.py:136
  237.5 2.4 fusion.11
  239.9 63.3 %conditional.7 = (f32[1,1,128,64]{2,3,1,0:T(8,128)}) conditional(s32[]{:T(128)} %convert_element_type.149, f32[1,1,128,64]{2,3,1,0:T(8,128)} %get-tuple-element.809, (s32[]{:T(128)}, s32[]{:T(128)}, bf16[4096,1,128]{2,0,1:T(8,128)(2,1)}, bf16[1,1,128,64]{3,2,1,0:T(8,128)(2,1)S(1)}, bf16[4096,1,2]{0,2,1:T(2,128)(2,1)S(1)}, ...), branch_computations={%region_7.7_spmd, %region_8.9_spmd} | conditional | flops 46151764 | bytes 16168209 | solution.py:142
  240.2 1.4 add.310
  241.6 1.0 dynamic-slice_bitcast_fusion.1
  244.9 54.7 %reduce_window_sum.22 = f32[1,2,64,16,64]{4,3,2,1,0:T(8,128)S(1)} reduce-window(f32[1,2,64,16,64]{4,3,2,1,0:T(8,128)S(1)} %fusion.13, f32[]{:T(128)} %constant.213.clone), window={size=1x1x1x1x64 pad=0_0x0_0x0_0x0_0x0_63}, to_apply=%region_9.8 | reduce-window | flops 8257536 | bytes 1048580 | tf_op jit(solution)/shard_map/while/body/eval_jaxpr/cond/branch_1_fun/reduce_window_sum | solution.py:136
  300.8 2.4 fusion.11
  303.2 63.3 %conditional.7 = (f32[1,1,128,64]{2,3,1,0:T(8,128)}) conditional(s32[]{:T(128)} %convert_element_type.149, f32[1,1,128,64]{2,3,1,0:T(8,128)} %get-tuple-element.809, (s32[]{:T(128)}, s32[]{:T(128)}, bf16[4096,1,128]{2,0,1:T(8,128)(2,1)}, bf16[1,1,128,64]{3,2,1,0:T(8,128)(2,1)S(1)}, bf16[4096,1,2]{0,2,1:T(2,128)(2,1)S(1)}, ...), branch_computations={%region_7.7_spmd, %region_8.9_spmd} | conditional | flops 46151764 | bytes 16168209 | solution.py:142
  303.5 1.4 add.310
  304.9 1.0 dynamic-slice_bitcast_fusion.1
  307.6 0.7 fusion.13
  308.3 54.7 %reduce_window_sum.22 = f32[1,2,64,16,64]{4,3,2,1,0:T(8,128)S(1)} reduce-window(f32[1,2,64,16,64]{4,3,2,1,0:T(8,128)S(1)} %fusion.13, f32[]{:T(128)} %constant.213.clone), window={size=1x1x1x1x64 pad=0_0x0_0x0_0x0_0x0_63}, to_apply=%region_9.8 | reduce-window | flops 8257536 | bytes 1048580 | tf_op jit(solution)/shard_map/while/body/eval_jaxpr/cond/branch_1_fun/reduce_window_sum | solution.py:136
  364.2 2.4 fusion.11
  366.6 63.3 %conditional.7 = (f32[1,1,128,64]{2,3,1,0:T(8,128)}) conditional(s32[]{:T(128)} %convert_element_type.149, f32[1,1,128,64]{2,3,1,0:T(8,128)} %get-tuple-element.809, (s32[]{:T(128)}, s32[]{:T(128)}, bf16[4096,1,128]{2,0,1:T(8,128)(2,1)}, bf16[1,1,128,64]{3,2,1,0:T(8,128)(2,1)S(1)}, bf16[4096,1,2]{0,2,1:T(2,128)(2,1)S(1)}, ...), branch_computations={%region_7.7_spmd, %region_8.9_spmd} | conditional | flops 46151764 | bytes 16168209 | solution.py:142
  366.8 1.4 add.310
  368.3 1.0 dynamic-slice_bitcast_fusion.1
  370.9 0.7 fusion.13
  371.6 54.7 %reduce_window_sum.22 = f32[1,2,64,16,64]{4,3,2,1,0:T(8,128)S(1)} reduce-window(f32[1,2,64,16,64]{4,3,2,1,0:T(8,128)S(1)} %fusion.13, f32[]{:T(128)} %constant.213.clone), window={size=1x1x1x1x64 pad=0_0x0_0x0_0x0_0x0_63}, to_apply=%region_9.8 | reduce-window | flops 8257536 | bytes 1048580 | tf_op jit(solution)/shard_map/while/body/eval_jaxpr/cond/branch_1_fun/reduce_window_sum | solution.py:136
  427.5 2.4 fusion.11
  429.9 0.8 convert_element_type.94
  431.4 31.3 %all_to_all.10 = bf16[8,64,2048]{2,1,0:T(8,128)(2,1)S(1)} all-to-all(bf16[8,64,2048]{2,1,0:T(8,128)(2,1)S(1)} %broadcast_in_dim.36), channel_id=1, replica_groups=mesh['sp'=64,'tp'=8] {'tp'}, dimensions={0} | all-to-all | bytes 4194304 | tf_op jit(solution)/shard_map/all_to_all | solution.py:23
  463.9 4.1 fusion.26
  468.0 3.4 all-to-all-start.1
  471.4 7.4 %all-to-all-done.1 = bf16[8,8,2048]{2,1,0:T(8,128)(2,1)S(1)} async-done(((bf16[8,8,2048]{2,1,0:T(8,128)(2,1)}), bf16[8,8,2048]{2,1,0:T(8,128)(2,1)S(1)}, u32[]{:S(2)}, u32[]{:S(2)}) %all-to-all-start.1) | async-done | bytes 262176 | tf_op jit(solution)/shard_map/all_to_all | solution.py:38
  (146 shorter events, 22.8 us)
Async XLA Ops:
  6.5 424.4 %copy-start = (bf16[128,2048]{1,0:T(8,128)(2,1)S(1)}, bf16[128,2048]{1,0:T(8,128)(2,1)}, u32[]{:S(2)}) copy-start(bf16[128,2048]{1,0:T(8,128)(2,1)} %param.20) | copy-start | bytes 1572868
  6.5 141.5 %all-gather.4.cloned.1.call-start = ((), (), s32[]{:S(2)}) async-start(), calls=%async_computation.2 | async-start | bytes 2129920 | tf_op jit(solution)/shard_map/all_gather | solution.py:17
  8.7 455.1 %all-gather.6.cloned.1.call-start = ((), (), s32[]{:S(2)}) async-start(), calls=%async_computation.3 | async-start | bytes 2129920 | tf_op jit(solution)/shard_map/all_gather | solution.py:165
  9.5 454.4 %all-gather.8.cloned.1.call-start = ((), (), s32[]{:S(2)}) async-start(), calls=%async_computation.4 | async-start | bytes 2129920 | tf_op jit(solution)/shard_map/all_gather | solution.py:171
  236.3 1.2 copy-start.1
  299.7 1.2 copy-start.1
  363.0 1.2 copy-start.1
  426.4 1.2 copy-start.1
  462.7 1.0 copy-start.2
  462.7 1.2 copy-start.3
  468.0 10.8 %all-to-all-start.1 = ((bf16[8,8,2048]{2,1,0:T(8,128)(2,1)}), bf16[8,8,2048]{2,1,0:T(8,128)(2,1)S(1)}, u32[]{:S(2)}, u32[]{:S(2)}) async-start(bf16[8,8,2048]{2,1,0:T(8,128)(2,1)} %fusion.26), calls=%async_computation.1 | async-start | bytes 524288 | tf_op jit(solution)/shard_map/all_to_all | solution.py:38
Sparse Core Ops, SparseCore 0:
  10.3 137.7 all-gather.3
  151.0 137.6 all-gather.5
  291.6 137.2 all-gather.7
where the time goes:
time: 488 us; the launch traced here: 486 us
  other arithmetic  242 us (50%)
  waiting for transfers between devices  146 us (30%)
  local copies, waits for them, and re-layouts  33.3 us (7%)
  blocking collectives  31.3 us (6%)
  matrix products  15.7 us (3%)
  between operations  13.2 us (3%)
    another operation x4, other arithmetic, out_compute(): within = lax.cumsum(split_pass, axis=4, reverse=True) - split_pass  219 us
    all_gather x1, waiting for transfers between devices, side_by_side(): out = lax.all_gather(both, axis, axis=dim, tiled=True)  137 us
    all_to_all x1, blocking collectives, from_everyone(): return lax.all_to_all(copies, axis, split_axis=0, concat_axis=0, tiled=True)  31.3 us
    reduce_sum x4, other arithmetic, sum_compute(): block_sums = log_pass.reshape(seq_count, head_count, row_count, shard_gro...  14.6 us
  transfers between devices with their start and end apart: 4, of which 2 were waited for; matrix products, arithmetic and copies ran while one was open for 58% of the time, Pallas kernels for 0%

commit v1 on v0

v1 whole, which is shorter than its diff:
```python
import jax
import jax.numpy as jnp
from jax import lax
from jax.experimental import pallas as pl
from jax.experimental.pallas import tpu as pltpu
from jax.sharding import PartitionSpec as P

MESH = pl.DeviceIdType.MESH
NZ, NY, NX, NC = 16, 4, 4, 2
NCHIP = NX * NY
HEAD = 64
ROWS = 64
D = 2048
HALF = D // 2
EPSILON = 1e-06
LOG2E = 1.4426950408889634
UP_STEPS, DOWN_STEPS = 8, 7


def nn(a, b):
    return lax.dot_general(a, b, (((1,), (0,)), ((), ())), preferred_element_type=jnp.float32)


def nt(a, b):
    return lax.dot_general(a, b, (((1,), (1,)), ((), ())), preferred_element_type=jnp.float32)


def tn(a, b):
    return lax.dot_general(a, b, (((0,), (0,)), ((), ())), preferred_element_type=jnp.float32)


def kernel(
    tok_ref, q_ref, kv_ref, bias_ref, wo_ref, gain_ref, up_ref, down_ref, out_ref,
    kvall, wbuf, wcat, pbuf, prec, xbuf, e1, e1r, own, e2, erec,
    u_hi, s_hi, u_lo, s_lo,
    kv_s, kv_r, yf_s, yf_r, we_s, we_r, w_s, w_r, p_s, p_r, x_s, x_r, xd_s, xd_r, e1_s, e1_r, e_s, e_r,
):
    sp = lax.axis_index("sp")
    tp = lax.axis_index("tp")
    z, y = sp // NY, sp % NY
    x, c = tp // NC, tp % NC
    chip = y * NX + x
    z_next, z_prev = (z + 1) % NZ, (z + NZ - 1) % NZ
    sibling = (sp, x * NC + 1 - c)

    def chip_at(r, core):
        dy, dx = r // NX, r % NX
        return (z * NY + (y + dy) % NY, ((x + dx) % NX) * NC + core)

    def rdma(src, dst, send, recv, device):
        return pltpu.make_async_remote_copy(
            src_ref=src, dst_ref=dst, send_sem=send, recv_sem=recv, device_id=device, device_id_type=MESH
        )

    barrier = pltpu.get_barrier_semaphore()
    peers = [(z_next * NY + y, tp), (z_prev * NY + y, tp), sibling]
    peers += [chip_at(r, c) for r in range(1, NCHIP)]
    peers += [chip_at(r, 1 - c) for r in range(1, NX)]
    for peer in peers:
        pl.semaphore_signal(barrier, inc=1, device_id=peer, device_id_type=MESH)

    kvall[z, y, 0:ROWS, :] = kv_ref[...]
    bias = bias_ref[...].astype(jnp.float32)
    bias = jnp.concatenate([bias, jnp.zeros((14, HEAD), jnp.float32)], axis=0)
    bias = jnp.concatenate([bias, jnp.zeros((16, HEAD), jnp.float32)], axis=1)
    kvall[z, y, ROWS : ROWS + 16, :] = bias.astype(jnp.bfloat16)
    u_hi[...] = jnp.zeros_like(u_hi)
    u_lo[...] = jnp.zeros_like(u_lo)
    s_hi[...] = jnp.zeros_like(s_hi)
    s_lo[...] = jnp.zeros_like(s_lo)

    pl.semaphore_wait(barrier, len(peers))

    def kv_up(k):
        slot = kvall.at[(z - k + 1 + NZ) % NZ, y]
        return rdma(slot, slot, kv_s.at[0, k], kv_r.at[0, k], (z_next * NY + y, tp))

    def kv_down(k):
        slot = kvall.at[(z + k - 1) % NZ, y]
        return rdma(slot, slot, kv_s.at[1, k], kv_r.at[1, k], (z_prev * NY + y, tp))

    def kv_hand(direction, k, p, d):
        slot = kvall.at[p, y]
        return rdma(
            slot, slot, yf_s.at[direction, k, d], yf_r.at[direction, k, d], (z * NY + (y + d) % NY, tp)
        )

    def up_sends(k):
        return (k <= UP_STEPS) & (z - k + 1 >= 0) & (z <= NZ - 2)

    def up_arrives(k):
        return (k <= UP_STEPS) & (z - k >= 0)

    def down_sends(k):
        return (k <= DOWN_STEPS) & ((z + k - 1) % NZ <= DOWN_STEPS - 1)

    def down_arrives(k):
        return (k <= DOWN_STEPS) & ((z + k) % NZ <= DOWN_STEPS - 1)

    def down_used(k):
        return (k <= DOWN_STEPS) & (z + k >= NZ)

    @pl.when(up_sends(1))
    def _():
        kv_up(1).start()

    @pl.when(down_sends(1))
    def _():
        kv_down(1).start()

    for d in range(1, NY):
        kv_hand(0, 0, z, d).start()

    def w_hand(d, which):
        src = (up_ref, down_ref)[which]
        to = (y + d) % NY
        return rdma(
            src.at[:, pl.ds(pl.multiple_of(to * 128, 128), 128)],
            wbuf.at[z, which, pl.ds(pl.multiple_of(y * 32, 32), 32), :],
            we_s.at[d, which], we_r.at[d, which], (z * NY + to, tp),
        )

    for d in range(1, NY):
        for which in range(2):
            w_hand(d, which).start()
    for which in range(2):
        src = (up_ref, down_ref)[which]
        wbuf[z, which, pl.ds(pl.multiple_of(y * 32, 32), 32), :] = src[
            :, pl.ds(pl.multiple_of(y * 128, 128), 128)
        ]

    def w_copy(direction, k):
        p = (z - k + 1 + NZ) % NZ if direction == 0 else (z + k - 1) % NZ
        to = (z_next, z_prev)[direction]
        slot = wbuf.at[p]
        return rdma(slot, slot, w_s.at[direction, k], w_r.at[direction, k], (to * NY + y, tp))

    def w_first():
        for d in range(1, NY):
            for which in range(2):
                w_hand(d, which).wait_recv()
        w_copy(0, 1).start()
        w_copy(1, 1).start()

    def w_step(k):
        w_copy(0, k).wait_recv()
        if k <= DOWN_STEPS:
            w_copy(1, k).wait_recv()
        if k + 1 <= UP_STEPS:
            w_copy(0, k + 1).start()
        if k + 1 <= DOWN_STEPS:
            w_copy(1, k + 1).start()

    q = q_ref[...].astype(jnp.float32) * 0.125
    queries = jnp.concatenate([q[:, :HEAD], q[:, HEAD:]], axis=0).astype(jnp.bfloat16)
    pick = lax.broadcasted_iota(jnp.int32, (16, 128), 1) // HEAD
    pick = (pick == lax.broadcasted_iota(jnp.int32, (16, 128), 0)).astype(jnp.float32).astype(jnp.bfloat16)
    later = lax.broadcasted_iota(jnp.int32, (256, 256), 1) > lax.broadcasted_iota(jnp.int32, (256, 256), 0)
    later = later.astype(jnp.float32).astype(jnp.bfloat16)

    def attend(p, diagonal, carry):
        parts = []
        for b in range(NY):
            keys = kvall[p, b, 0:ROWS, 0:HEAD]
            biases = kvall[p, b, ROWS : ROWS + 16, 0:HEAD]
            parts.append(nt(keys, queries) + tn(biases, pick))
        score = jnp.concatenate(parts, axis=0) * LOG2E
        tail = jnp.log2(1.0 + jnp.exp2(-jnp.abs(score)))
        log_pass = -jnp.maximum(score, 0.0) - tail
        log_stop = jnp.minimum(score, 0.0) - tail
        if diagonal:
            key_at = lax.broadcasted_iota(jnp.int32, (256, 128), 0)
            query_at = y * ROWS + lax.broadcasted_iota(jnp.int32, (256, 128), 1) % HEAD
            strict = key_at < query_at
            log_pass = jnp.where(strict, log_pass, 0.0)
        high = log_pass.astype(jnp.bfloat16)
        low = (log_pass - high.astype(jnp.float32)).astype(jnp.bfloat16)
        after = nn(later, jnp.concatenate([high, low], axis=1))
        after = after[:, :128] + after[:, 128:]
        total = after[0:1, :] + log_pass[0:1, :]
        weights = jnp.exp2(log_stop + (after + carry))
        if diagonal:
            weights = jnp.where(strict, weights, 0.0)
        weights = weights.astype(jnp.bfloat16)
        values = jnp.concatenate([kvall[p, b, 0:ROWS, HEAD:128] for b in range(NY)], axis=0)
        return tn(values, weights), total

    def attend_high(p, diagonal):
        carry = s_hi[0:1, :]
        part, total = attend(p, diagonal, carry)
        u_hi[...] += part
        s_hi[0:1, :] = carry + total

    def attend_low(p):
        part, total = attend(p, False, 0.0)
        u_lo[...] = u_lo[...] * jnp.exp2(total) + part
        s_lo[0:1, :] += total

    def step(k, unused):
        @pl.when(up_arrives(k))
        def _():
            kv_up(k).wait_recv()

        @pl.when(up_sends(k + 1))
        def _():
            kv_up(k + 1).start()

        @pl.when(up_arrives(k))
        def _():
            for d in range(1, NY):
                kv_hand(0, k, (z - k + NZ) % NZ, d).start()

        @pl.when(down_arrives(k))
        def _():
            kv_down(k).wait_recv()

        @pl.when(down_sends(k + 1))
        def _():
            kv_down(k + 1).start()

        @pl.when(down_used(k))
        def _():
            for d in range(1, NY):
                kv_hand(1, k, (z + k) % NZ, d).start()

        @pl.when(k == 2)
        def _():
            w_first()

        for w in range(1, 4):
            @pl.when(k == 2 * w + 2)
            def _():
                w_step(w)

        @pl.when(k == 1)
        def _():
            for d in range(1, NY):
                kv_hand(0, 0, z, d).wait_recv()
            attend_high(z, True)

        @pl.when((k > 1) & (z - k + 1 >= 0))
        def _():
            p = (z - k + 1 + NZ) % NZ
            for d in range(1, NY):
                kv_hand(0, k - 1, p, d).wait_recv()
            attend_high(p, False)

        @pl.when((k > 1) & down_used(k - 1))
        def _():
            p = (z + k - 1) % NZ
            for d in range(1, NY):
                kv_hand(1, k - 1, p, d).wait_recv()
            attend_low(p)

        return unused

    lax.fori_loop(1, UP_STEPS + 2, step, 0)

    mixed = u_hi[...] + u_lo[...] * jnp.exp2(s_hi[0:1, :])
    mixed = mixed.T.astype(jnp.bfloat16)
    w_step(4)

    partial = nn(mixed[:ROWS], wo_ref[0:HEAD, :]) + nn(mixed[ROWS:], wo_ref[HEAD:, :])
    partial = partial.reshape(8, 8, D)
    pbuf[...] = jnp.concatenate([partial[:, :, :HALF], partial[:, :, HALF:]], axis=1).astype(jnp.bfloat16)

    def p_copy(r):
        to = (tp + r) % 8
        return rdma(pbuf.at[to], prec.at[r], p_s.at[r], p_r.at[r], (sp, to))

    for r in range(1, 8):
        p_copy(r).start()
    w_step(5)
    projected = pbuf[tp].astype(jnp.float32)
    for r in range(1, 8):
        p_copy(r).wait_recv()
        projected = projected + prec[r].astype(jnp.float32)
    projected = jnp.concatenate([projected[:8], projected[8:]], axis=1)
    residual = (tok_ref[...].astype(jnp.float32) + projected).astype(jnp.bfloat16).astype(jnp.float32)
    factor = lax.rsqrt(jnp.mean(residual * residual, axis=-1, keepdims=True) + EPSILON)
    normed = residual * factor * gain_ref[...]
    xbuf[c, chip] = jnp.concatenate([normed[:, :HALF], normed[:, HALF:]], axis=0).astype(jnp.bfloat16)

    def x_copy(r):
        slot = xbuf.at[c, chip]
        return rdma(slot, slot, x_s.at[r], x_r.at[r], chip_at(r, c))

    def x_pass(r):
        dy, dx = r // NX, r % NX
        source = ((y + NY - dy) % NY) * NX + (x + NX - dx) % NX
        slot = xbuf.at[c, source]
        return rdma(slot, slot, xd_s.at[r], xd_r.at[r], sibling)

    order = sorted(range(1, NCHIP), key=lambda r: min(r // NX, NY - r // NX) + min(r % NX, NX - r % NX))
    for r in reversed(order):
        x_copy(r).start()
    x_pass(0).start()
    w_step(6)
    w_step(7)
    for r in order:
        x_copy(r).wait_recv()
        x_pass(r).start()
    w_step(8)
    for p in range(8):
        wcat[p * 128 : (p + 1) * 128, 0:128] = wbuf[p, 0]
        wcat[p * 128 : (p + 1) * 128, 128:256] = wbuf[p + 8, 0]
    for r in range(NCHIP):
        x_pass(r).wait_recv()

    def hidden_of(core):
        both = nn(xbuf[core].reshape(NCHIP * 16, HALF), wcat[...]).reshape(NCHIP, 16, 256)
        h = both[:, :8, :128] + both[:, 8:, 128:]
        h = jnp.maximum(h.reshape(NCHIP * 8, 128), 0.0)
        return (h * h).astype(jnp.bfloat16)

    def update_of(h, target, dtype):
        for p in range(8):
            w = jnp.concatenate([wbuf[p, 1], wbuf[p + 8, 1]], axis=0)
            o = nt(h, w).reshape(NCHIP, 8, 256)
            target[:, :, p * 128 : (p + 1) * 128] = jnp.concatenate(
                [o[:, :, :128], o[:, :, 128:]], axis=1
            ).astype(dtype)

    update_of(hidden_of(1 - c), e1, jnp.bfloat16)
    swap = rdma(e1, e1r, e1_s, e1_r, sibling)
    swap.start()
    update_of(hidden_of(c), own, jnp.float32)
    swap.wait_recv()

    def e_copy(r):
        dy, dx = r // NX, r % NX
        target = ((y + dy) % NY) * NX + (x + dx) % NX
        return rdma(e2.at[target], erec.at[r], e_s.at[r], e_r.at[r], chip_at(r, c))

    e2[...] = (own[...] + e1r[...].astype(jnp.float32)).astype(jnp.bfloat16)
    for r in reversed(order):
        e_copy(r).start()
    update = own[chip] + e1r[chip].astype(jnp.float32)
    for r in order:
        e_copy(r).wait_recv()
        update = update + erec[r].astype(jnp.float32)
    update = jnp.concatenate([update[:8], update[8:]], axis=1)
    out_ref[...] = (residual + update).astype(jnp.bfloat16)

    def drain(k, unused):
        @pl.when(up_sends(k))
        def _():
            kv_up(k).wait_send()

        @pl.when(down_sends(k))
        def _():
            kv_down(k).wait_send()

        @pl.when(up_arrives(k))
        def _():
            for d in range(1, NY):
                kv_hand(0, k, (z - k + NZ) % NZ, d).wait_send()

        @pl.when(down_used(k))
        def _():
            for d in range(1, NY):
                kv_hand(1, k, (z + k) % NZ, d).wait_send()

        return unused

    lax.fori_loop(1, UP_STEPS + 1, drain, 0)
    for d in range(1, NY):
        kv_hand(0, 0, z, d).wait_send()
        for which in range(2):
            w_hand(d, which).wait_send()
    for k in range(1, UP_STEPS + 1):
        w_copy(0, k).wait_send()
    for k in range(1, DOWN_STEPS + 1):
        w_copy(1, k).wait_send()
    for r in range(1, 8):
        p_copy(r).wait_send()
    for r in range(NCHIP):
        x_pass(r).wait_send()
    for r in range(1, NCHIP):
        x_copy(r).wait_send()
        e_copy(r).wait_send()
    swap.wait_send()


def body(tokens, queries, key_values, stop_bias, out_proj, norm_gain, up_proj, down_proj):
    tp = lax.axis_index("tp")
    own_tokens = lax.dynamic_slice_in_dim(tokens, tp * 8, 8, 0).reshape(8, D)
    bf, f32 = jnp.bfloat16, jnp.float32
    dma = pltpu.SemaphoreType.DMA
    out = pl.pallas_call(
        kernel,
        out_shape=jax.ShapeDtypeStruct((8, D), bf),
        in_specs=[pl.BlockSpec(memory_space=pltpu.VMEM)] * 8,
        out_specs=pl.BlockSpec(memory_space=pltpu.VMEM),
        scratch_shapes=[
            pltpu.VMEM((NZ, NY, ROWS + 16, 128), bf),
            pltpu.VMEM((NZ, 2, 128, 128), bf),
            pltpu.VMEM((HALF, 256), bf),
            pltpu.VMEM((8, 16, HALF), bf),
            pltpu.VMEM((8, 16, HALF), bf),
            pltpu.VMEM((NC, NCHIP, 16, HALF), bf),
            pltpu.VMEM((NCHIP, 16, HALF), bf),
            pltpu.VMEM((NCHIP, 16, HALF), bf),
            pltpu.VMEM((NCHIP, 16, HALF), f32),
            pltpu.VMEM((NCHIP, 16, HALF), bf),
            pltpu.VMEM((NCHIP, 16, HALF), bf),
            pltpu.VMEM((HEAD, 128), f32),
            pltpu.VMEM((8, 128), f32),
            pltpu.VMEM((HEAD, 128), f32),
            pltpu.VMEM((8, 128), f32),
            dma((2, 9)), dma((2, 9)),
            dma((2, 9, 4)), dma((2, 9, 4)),
            dma((4, 2)), dma((4, 2)),
            dma((2, 9)), dma((2, 9)),
            dma((8,)), dma((8,)),
            dma((NCHIP,)), dma((NCHIP,)),
            dma((NCHIP,)), dma((NCHIP,)),
            dma(()), dma(()),
            dma((NCHIP,)), dma((NCHIP,)),
        ],
        compiler_params=pltpu.CompilerParams(
            collective_id=0, has_side_effects=True, vmem_limit_bytes=40 * 1024 * 1024
        ),
        name="layer",
    )(
        own_tokens,
        queries.reshape(ROWS, 128),
        key_values.reshape(ROWS, 128),
        stop_bias.reshape(ROWS, 2).T,
        out_proj,
        norm_gain.reshape(1, D),
        up_proj,
        down_proj.T,
    )
    return out.reshape(8, 1, D)


def solution(mesh):
    return jax.shard_map(
        body,
        mesh=mesh,
        in_specs=(
            P("sp", None, None),
            P("sp", None, "tp"),
            P("sp", None, "tp"),
            P("sp", None, "tp"),
            P("tp", None),
            P(),
            P("sp", "tp"),
            P("tp", "sp"),
        ),
        out_specs=P(("sp", "tp"), None, None),
        check_vma=False,
    )
```

time: 488 us -> 77.5 us (0.16)
  the two profiles are of different devices: /device:TPU:480 before, /device:TPU:1 now
where the time goes in v1:
time: 77.5 us; the launch traced here: 77.2 us
  Pallas kernels  72.4 us (93%)
  local copies, waits for them, and re-layouts  4.78 us (6%)
    pallas_call x1, Pallas kernels, body(): pl.pallas_call(kernel, out_shape=jax.ShapeDtypeStruct((8, D), bf), in_spe...  72.4 us
    unnamed x17, local copies, waits for them, and re-layouts  4.78 us

profile of v1, /device:TPU:1, one launch (start us, length us, event | category | flops | bytes accessed | tf_op | source)
XLA Modules:
  0.0 77.2 jit_solution(9251177052753777409)
XLA Ops:
  0.0 0.0 copy-start
  0.0 0.0 copy-start.4
  0.0 0.9 %copy-done = bf16[64,1,2048]{2,0,1:T(8,128)(2,1)S(1)} copy-done((bf16[64,1,2048]{2,0,1:T(8,128)(2,1)S(1)}, bf16[64,1,2048]{2,0,1:T(8,128)(2,1)}, u32[]{:S(2)}) %copy-start) | copy-done | bytes 262168
  1.0 0.0 copy-start.2
  1.0 0.0 copy-start.3
  1.0 0.0 copy-start.7
  1.0 0.0 copy-done.4
  1.0 0.7 copy-done.2
  1.7 0.0 copy-done.3
  1.7 0.0 copy-done.7
  1.7 0.0 copy-start.1
  1.7 1.0 %copy-done.1 = bf16[128,2048]{1,0:T(8,128)(2,1)S(1)} copy-done((bf16[128,2048]{1,0:T(8,128)(2,1)S(1)}, bf16[128,2048]{1,0:T(8,128)(2,1)}, u32[]{:S(2)}) %copy-start.1) | copy-done | bytes 524312
  2.8 0.0 copy-start.5
  2.8 0.7 copy-done.5
  3.5 0.0 copy-start.6
  3.5 0.7 copy-done.6
  4.2 72.4 %layer.1 = bf16[8,2048]{1,0:T(8,128)(2,1)S(1)} custom-call(bf16[8,2048]{1,0:T(8,128)(2,1)S(1)} %dynamic-slice_bitcast_fusion.tok_ref, bf16[64,128]{1,0:T(8,128)(2,1)S(1)} %bitcast.12, bf16[64,128]{1,0:T(8,128)(2,1)S(1)} %bitcast.13, bf16[2,64]{1,0:T(2,128)(2,1)S(1)} %bitcast.15, bf16[128,2048]{1,0:T(8,128)(2,1)S(1)} %copy-done.1, f32[1,2048]{1,0:T(1,128)S(1)} %bitcast.14, ...), custom_call_target="tpu_custom_call" | custom-call | tf_op jit(solution)/shard_map/layer/pallas_call | solution.py:390
  76.6 0.6 copy.10
  (1 shorter events, 0.0 us)
Async XLA Ops:
  0.0 1.0 %copy-start = (bf16[64,1,2048]{2,0,1:T(8,128)(2,1)S(1)}, bf16[64,1,2048]{2,0,1:T(8,128)(2,1)}, u32[]{:S(2)}) copy-start(bf16[64,1,2048]{2,0,1:T(8,128)(2,1)} %param.8) | copy-start | bytes 786436
  0.0 1.0 %copy-start.4 = (bf16[64,1,128]{2,0,1:T(8,128)(2,1)S(1)}, bf16[64,1,128]{2,0,1:T(8,128)(2,1)}, u32[]{:S(2)}) copy-start(bf16[64,1,128]{2,0,1:T(8,128)(2,1)} %param.9) | copy-start | bytes 49156
  1.0 0.8 copy-start.2
  1.0 0.8 copy-start.3
  1.0 0.8 %copy-start.7 = (bf16[64,1,2]{0,2,1:T(2,128)(2,1)S(1)}, bf16[64,1,2]{0,2,1:T(2,128)(2,1)}, u32[]{:S(2)}) copy-start(bf16[64,1,2]{0,2,1:T(2,128)(2,1)} %param.11) | copy-start | bytes 772
  1.7 1.0 %copy-start.1 = (bf16[128,2048]{1,0:T(8,128)(2,1)S(1)}, bf16[128,2048]{1,0:T(8,128)(2,1)}, u32[]{:S(2)}) copy-start(bf16[128,2048]{1,0:T(8,128)(2,1)} %wo_ref.1) | copy-start | bytes 1572868
  2.8 0.7 copy-start.5
  3.5 0.7 copy-start.6

commit v2 on v1

v2 whole, which is shorter than its diff:
```python
import jax
import jax.numpy as jnp
from jax import lax
from jax.experimental import pallas as pl
from jax.experimental.pallas import tpu as pltpu
from jax.sharding import PartitionSpec as P

MESH = pl.DeviceIdType.MESH
NZ, NY, NX, NC = 16, 4, 4, 2
NCHIP = NX * NY
HEAD = 64
ROWS = 64
D = 2048
HALF = D // 2
EPSILON = 1e-06
LOG2E = 1.4426950408889634
UP_STEPS, DOWN_STEPS = 8, 7


def nn(a, b):
    return lax.dot_general(a, b, (((1,), (0,)), ((), ())), preferred_element_type=jnp.float32)


def nt(a, b):
    return lax.dot_general(a, b, (((1,), (1,)), ((), ())), preferred_element_type=jnp.float32)


def tn(a, b):
    return lax.dot_general(a, b, (((0,), (0,)), ((), ())), preferred_element_type=jnp.float32)


def kernel(
    tok_hbm, q_hbm, kv_hbm, bias_hbm, wo_hbm, gain_hbm, up_hbm, down_hbm, out_ref,
    tok_ref, q_ref, bias_ref, wo_ref, gain_ref, up_ref, down_ref, in_s,
    kvall, wbuf, wcat, pbuf, prec, xbuf, e1, e1r, own, e2, erec,
    u_hi, s_hi, u_lo, s_lo,
    kv_s, kv_r, yf_s, yf_r, we_s, we_r, w_s, w_r, p_s, p_r, x_s, x_r, xd_s, xd_r, e1_s, e1_r, e_s, e_r,
):
    sp = lax.axis_index("sp")
    tp = lax.axis_index("tp")
    z, y = sp // NY, sp % NY
    x, c = tp // NC, tp % NC
    chip = y * NX + x
    sibling = (sp, x * NC + 1 - c)

    def chip_at(r, core):
        dy, dx = r // NX, r % NX
        return (z * NY + (y + dy) % NY, ((x + dx) % NX) * NC + core)

    def rdma(src, dst, send, recv, device):
        return pltpu.make_async_remote_copy(
            src_ref=src, dst_ref=dst, send_sem=send, recv_sem=recv, device_id=device, device_id_type=MESH
        )

    barrier = pltpu.get_barrier_semaphore()
    peers = [(((z + d) % NZ) * NY + y, tp) for d in (1, 2, NZ - 2, NZ - 1)] + [sibling]
    peers += [chip_at(r, c) for r in range(1, NCHIP)]
    peers += [chip_at(r, 1 - c) for r in range(1, NX)]
    for peer in peers:
        pl.semaphore_signal(barrier, inc=1, device_id=peer, device_id_type=MESH)

    loads = [
        pltpu.make_async_copy(src, dst, in_s.at[i])
        for i, (src, dst) in enumerate(
            (
                (kv_hbm, kvall.at[z, y, 0:ROWS, :]),
                (bias_hbm, bias_ref),
                (up_hbm, up_ref),
                (down_hbm, down_ref),
                (q_hbm, q_ref),
                (wo_hbm, wo_ref),
                (tok_hbm.at[pl.ds(pl.multiple_of(tp * 8, 8), 8), :], tok_ref),
                (gain_hbm, gain_ref),
            )
        )
    ]
    for load in loads:
        load.start()

    loads[1].wait()
    bias = bias_ref[...].astype(jnp.float32)
    bias = jnp.concatenate([bias, jnp.zeros((14, HEAD), jnp.float32)], axis=0)
    bias = jnp.concatenate([bias, jnp.zeros((16, HEAD), jnp.float32)], axis=1)
    kvall[z, y, ROWS : ROWS + 16, :] = bias.astype(jnp.bfloat16)
    u_hi[...] = jnp.zeros_like(u_hi)
    u_lo[...] = jnp.zeros_like(u_lo)
    s_hi[...] = jnp.zeros_like(s_hi)
    s_lo[...] = jnp.zeros_like(s_lo)

    loads[0].wait()
    pl.semaphore_wait(barrier, len(peers))

    def along(buffer, send, recv, direction, d):
        odd = d % 2
        held = d - 2 + odd
        hop = 2 - odd
        if direction == 0:
            p, to = (z - held + NZ) % NZ, (z + hop) % NZ
        else:
            p, to = (z + held) % NZ, (z - hop + NZ) % NZ
        slot = buffer(p)
        return rdma(slot, slot, send.at[direction, d], recv.at[direction, d], (to * NY + y, tp))

    def kv_copy(direction, d):
        return along(lambda p: kvall.at[p, y], kv_s, kv_r, direction, d)

    def kv_hand(direction, k, p, d):
        slot = kvall.at[p, y]
        return rdma(
            slot, slot, yf_s.at[direction, k, d], yf_r.at[direction, k, d], (z * NY + (y + d) % NY, tp)
        )

    def used(direction, d):
        return (z - d >= 0) if direction == 0 else (z + d >= NZ) & (d <= DOWN_STEPS)

    def place(direction, d):
        return (z - d + NZ) % NZ if direction == 0 else (z + d) % NZ

    def even_sends(direction, d):
        if direction == 0:
            return (d <= UP_STEPS) & (z - d + 2 >= 0) & (z + 2 < NZ)
        return (d <= DOWN_STEPS) & ((z + d - 2) % NZ < DOWN_STEPS)

    def even_arrives(direction, d):
        if direction == 0:
            return (d <= UP_STEPS) & (z - d >= 0)
        return (d <= DOWN_STEPS) & ((z + d) % NZ < DOWN_STEPS)

    def odd_sends(direction, d):
        if direction == 0:
            return (d <= UP_STEPS) & (z - d + 1 >= 0) & (z + 1 < NZ)
        return (d <= DOWN_STEPS) & ((z + NZ - 1) % NZ + d >= NZ)

    def odd_arrives(direction, d):
        return (d <= UP_STEPS) & used(direction, d)

    def kv_stage_sends(direction, j):
        @pl.when(even_sends(direction, 2 * j))
        def _():
            kv_copy(direction, 2 * j).start()

        @pl.when(odd_sends(direction, 2 * j - 1))
        def _():
            kv_copy(direction, 2 * j - 1).start()

    kv_stage_sends(0, 1)
    kv_stage_sends(1, 1)
    for d in range(1, NY):
        kv_hand(0, 0, z, d).start()

    def w_hand(d, which):
        src = (up_ref, down_ref)[which]
        to = (y + d) % NY
        return rdma(
            src.at[:, pl.ds(pl.multiple_of(to * 128, 128), 128)],
            wbuf.at[z, which, pl.ds(pl.multiple_of(y * 32, 32), 32), :],
            we_s.at[d, which], we_r.at[d, which], (z * NY + to, tp),
        )

    loads[2].wait()
    loads[3].wait()
    for d in range(1, NY):
        for which in range(2):
            w_hand(d, which).start()
    for which in range(2):
        src = (up_ref, down_ref)[which]
        wbuf[z, which, pl.ds(pl.multiple_of(y * 32, 32), 32), :] = src[
            :, pl.ds(pl.multiple_of(y * 128, 128), 128)
        ]

    def w_copy(direction, d):
        return along(lambda p: wbuf.at[p], w_s, w_r, direction, d)

    def w_far(j):
        for direction, last in ((0, UP_STEPS), (1, DOWN_STEPS)):
            if 2 * j <= last:
                if j == 0:
                    if direction == 0:
                        for d in range(1, NY):
                            for which in range(2):
                                w_hand(d, which).wait_recv()
                else:
                    w_copy(direction, 2 * j).wait_recv()
            if 2 * j + 2 <= last:
                w_copy(direction, 2 * j + 2).start()

    def w_near(j):
        for direction, last in ((0, UP_STEPS), (1, DOWN_STEPS)):
            if 2 * j + 1 <= last:
                w_copy(direction, 2 * j + 1).start()

    def w_rest():
        for d in range(1, UP_STEPS, 2):
            w_copy(0, d).wait_recv()
            w_copy(1, d).wait_recv()

    loads[4].wait()
    q = q_ref[...].astype(jnp.float32) * 0.125
    queries = jnp.concatenate([q[:, :HEAD], q[:, HEAD:]], axis=0).astype(jnp.bfloat16)
    pick = lax.broadcasted_iota(jnp.int32, (16, 128), 1) // HEAD
    pick = (pick == lax.broadcasted_iota(jnp.int32, (16, 128), 0)).astype(jnp.float32).astype(jnp.bfloat16)
    later = lax.broadcasted_iota(jnp.int32, (256, 256), 1) > lax.broadcasted_iota(jnp.int32, (256, 256), 0)
    later = later.astype(jnp.float32).astype(jnp.bfloat16)

    def attend(p, diagonal, carry):
        parts = []
        for b in range(NY):
            keys = kvall[p, b, 0:ROWS, 0:HEAD]
            biases = kvall[p, b, ROWS : ROWS + 16, 0:HEAD]
            parts.append(nt(keys, queries) + tn(biases, pick))
        score = jnp.concatenate(parts, axis=0) * LOG2E
        tail = jnp.log2(1.0 + jnp.exp2(-jnp.abs(score)))
        log_pass = -jnp.maximum(score, 0.0) - tail
        log_stop = jnp.minimum(score, 0.0) - tail
        if diagonal:
            key_at = lax.broadcasted_iota(jnp.int32, (256, 128), 0)
            query_at = y * ROWS + lax.broadcasted_iota(jnp.int32, (256, 128), 1) % HEAD
            strict = key_at < query_at
            log_pass = jnp.where(strict, log_pass, 0.0)
        high = log_pass.astype(jnp.bfloat16)
        low = (log_pass - high.astype(jnp.float32)).astype(jnp.bfloat16)
        after = nn(later, jnp.concatenate([high, low], axis=1))
        after = after[:, :128] + after[:, 128:]
        total = after[0:1, :] + log_pass[0:1, :]
        weights = jnp.exp2(log_stop + (after + carry))
        if diagonal:
            weights = jnp.where(strict, weights, 0.0)
        weights = weights.astype(jnp.bfloat16)
        values = jnp.concatenate([kvall[p, b, 0:ROWS, HEAD:128] for b in range(NY)], axis=0)
        return tn(values, weights), total

    def attend_high(p, diagonal):
        carry = s_hi[0:1, :]
        part, total = attend(p, diagonal, carry)
        u_hi[...] += part
        s_hi[0:1, :] = carry + total

    def attend_low(p):
        part, total = attend(p, False, 0.0)
        u_lo[...] = u_lo[...] * jnp.exp2(total) + part
        s_lo[0:1, :] += total

    def step(j, unused):
        for direction in range(2):
            @pl.when(even_arrives(direction, 2 * j))
            def _():
                kv_copy(direction, 2 * j).wait_recv()

            kv_stage_sends(direction, j + 1)

            @pl.when((2 * j <= UP_STEPS) & used(direction, 2 * j))
            def _():
                for d in range(1, NY):
                    kv_hand(direction, 2 * j, place(direction, 2 * j), d).start()

            @pl.when(odd_arrives(direction, 2 * j - 1))
            def _():
                kv_copy(direction, 2 * j - 1).wait_recv()
                for d in range(1, NY):
                    kv_hand(direction, 2 * j - 1, place(direction, 2 * j - 1), d).start()

        @pl.when(j == 2)
        def _():
            w_far(0)

        @pl.when(j == 3)
        def _():
            w_near(0)

        @pl.when(j == 4)
        def _():
            w_far(1)

        @pl.when(j == 1)
        def _():
            for d in range(1, NY):
                kv_hand(0, 0, z, d).wait_recv()
            attend_high(z, True)

        for back in (3, 2):
            k = 2 * j - back

            @pl.when((k > 0) & used(0, k))
            def _():
                for d in range(1, NY):
                    kv_hand(0, k, place(0, k), d).wait_recv()
                attend_high(place(0, k), False)

            @pl.when((k > 0) & used(1, k))
            def _():
                for d in range(1, NY):
                    kv_hand(1, k, place(1, k), d).wait_recv()
                attend_low(place(1, k))

        return unused

    lax.fori_loop(1, UP_STEPS // 2 + 2, step, 0)
    w_near(1)
    w_far(2)

    for load in loads[5:]:
        load.wait()

    mixed = u_hi[...] + u_lo[...] * jnp.exp2(s_hi[0:1, :])
    mixed = mixed.T.astype(jnp.bfloat16)

    partial = nn(mixed[:ROWS], wo_ref[0:HEAD, :]) + nn(mixed[ROWS:], wo_ref[HEAD:, :])
    partial = partial.reshape(8, 8, D)
    pbuf[...] = jnp.concatenate([partial[:, :, :HALF], partial[:, :, HALF:]], axis=1).astype(jnp.bfloat16)

    def p_copy(r):
        to = (tp + r) % 8
        return rdma(pbuf.at[to], prec.at[r], p_s.at[r], p_r.at[r], (sp, to))

    for r in range(1, 8):
        p_copy(r).start()
    w_near(2)
    w_far(3)
    w_near(3)
    projected = pbuf[tp].astype(jnp.float32)
    for r in range(1, 8):
        p_copy(r).wait_recv()
        projected = projected + prec[r].astype(jnp.float32)
    projected = jnp.concatenate([projected[:8], projected[8:]], axis=1)
    residual = (tok_ref[...].astype(jnp.float32) + projected).astype(jnp.bfloat16).astype(jnp.float32)
    factor = lax.rsqrt(jnp.mean(residual * residual, axis=-1, keepdims=True) + EPSILON)
    normed = residual * factor * gain_ref[...]
    xbuf[c, chip] = jnp.concatenate([normed[:, :HALF], normed[:, HALF:]], axis=0).astype(jnp.bfloat16)

    def x_copy(r):
        slot = xbuf.at[c, chip]
        return rdma(slot, slot, x_s.at[r], x_r.at[r], chip_at(r, c))

    def x_pass(r):
        dy, dx = r // NX, r % NX
        source = ((y + NY - dy) % NY) * NX + (x + NX - dx) % NX
        slot = xbuf.at[c, source]
        return rdma(slot, slot, xd_s.at[r], xd_r.at[r], sibling)

    rows_order = (2, 1, 3, 0)
    for dy in rows_order:
        for dx in (2, 1, 3, 0):
            if dy or dx:
                x_copy(dy * NX + dx).start()
    x_pass(0).start()
    w_far(4)
    w_rest()
    for p in range(8):
        wcat[p * 128 : (p + 1) * 128, 0:128] = wbuf[p, 0]
        wcat[p * 128 : (p + 1) * 128, 128:256] = wbuf[p + 8, 0]

    def row_of(dy):
        return pl.ds(pl.multiple_of(((y + NY - dy) % NY) * NX, NX), NX)

    def swap(dy):
        rows = row_of(dy)
        return rdma(e1.at[rows], e1r.at[rows], e1_s.at[dy], e1_r.at[dy], sibling)

    def e_copy(r):
        dy, dx = r // NX, r % NX
        target = ((y + dy) % NY) * NX + (x + dx) % NX
        return rdma(e2.at[target], erec.at[r], e_s.at[r], e_r.at[r], chip_at(r, c))

    def feed_forward(dy):
        for dx in (1, 3, 2, 0):
            if dy or dx:
                x_copy(dy * NX + dx).wait_recv()
                x_pass(dy * NX + dx).start()
        for dx in range(NX):
            x_pass(dy * NX + dx).wait_recv()
        rows = row_of(dy)
        both = jnp.concatenate([xbuf[1 - c, rows], xbuf[c, rows]], axis=0).reshape(2 * NX * 16, HALF)
        both = nn(both, wcat[...]).reshape(2 * NX, 16, 256)
        h = both[:, :8, :128] + both[:, 8:, 128:]
        h = jnp.maximum(h.reshape(2 * NX * 8, 128), 0.0)
        h = (h * h).astype(jnp.bfloat16)
        for p in range(8):
            w = jnp.concatenate([wbuf[p, 1], wbuf[p + 8, 1]], axis=0)
            o = nt(h, w).reshape(2 * NX, 8, 256)
            o = jnp.concatenate([o[:, :, :128], o[:, :, 128:]], axis=1)
            e1[rows, :, p * 128 : (p + 1) * 128] = o[:NX].astype(jnp.bfloat16)
            own[rows, :, p * 128 : (p + 1) * 128] = o[NX:]
        swap(dy).start()

    def send_back(dy):
        swap(dy).wait_recv()
        rows = row_of(dy)
        e2[rows] = (own[rows] + e1r[rows].astype(jnp.float32)).astype(jnp.bfloat16)
        for dx in (2, 1, 3, 0):
            r = ((NY - dy) % NY) * NX + dx
            if r:
                e_copy(r).start()

    for n, dy in enumerate(rows_order):
        feed_forward(dy)
        if n:
            send_back(rows_order[n - 1])
    send_back(rows_order[-1])
    update = own[chip] + e1r[chip].astype(jnp.float32)
    for dy in rows_order:
        for dx in range(NX):
            r = ((NY - dy) % NY) * NX + dx
            if r:
                e_copy(r).wait_recv()
                update = update + erec[r].astype(jnp.float32)
    update = jnp.concatenate([update[:8], update[8:]], axis=1)
    out_ref[...] = (residual + update).astype(jnp.bfloat16)

    def drain(j, unused):
        for direction in range(2):
            @pl.when(even_sends(direction, 2 * j))
            def _():
                kv_copy(direction, 2 * j).wait_send()

            @pl.when(odd_sends(direction, 2 * j - 1))
            def _():
                kv_copy(direction, 2 * j - 1).wait_send()

            for k in (2 * j - 1, 2 * j):
                @pl.when(used(direction, k))
                def _():
                    for d in range(1, NY):
                        kv_hand(direction, k, place(direction, k), d).wait_send()

        return unused

    lax.fori_loop(1, UP_STEPS // 2 + 1, drain, 0)
    for d in range(1, NY):
        kv_hand(0, 0, z, d).wait_send()
        for which in range(2):
            w_hand(d, which).wait_send()
    for k in range(1, UP_STEPS + 1):
        w_copy(0, k).wait_send()
    for k in range(1, DOWN_STEPS + 1):
        w_copy(1, k).wait_send()
    for r in range(1, 8):
        p_copy(r).wait_send()
    for r in range(NCHIP):
        x_pass(r).wait_send()
    for r in range(1, NCHIP):
        x_copy(r).wait_send()
        e_copy(r).wait_send()
    for dy in range(NY):
        swap(dy).wait_send()


def body(tokens, queries, key_values, stop_bias, out_proj, norm_gain, up_proj, down_proj):
    bf, f32 = jnp.bfloat16, jnp.float32
    dma = pltpu.SemaphoreType.DMA
    out = pl.pallas_call(
        kernel,
        out_shape=jax.ShapeDtypeStruct((8, D), bf),
        in_specs=[pl.BlockSpec(memory_space=pltpu.HBM)] * 8,
        out_specs=pl.BlockSpec(memory_space=pltpu.VMEM),
        scratch_shapes=[
            pltpu.VMEM((8, D), bf),
            pltpu.VMEM((ROWS, 128), bf),
            pltpu.VMEM((2, HEAD), bf),
            pltpu.VMEM((128, D), bf),
            pltpu.VMEM((1, D), f32),
            pltpu.VMEM((32, 512), bf),
            pltpu.VMEM((32, 512), bf),
            dma((8,)),
            pltpu.VMEM((NZ, NY, ROWS + 16, 128), bf),
            pltpu.VMEM((NZ, 2, 128, 128), bf),
            pltpu.VMEM((HALF, 256), bf),
            pltpu.VMEM((8, 16, HALF), bf),
            pltpu.VMEM((8, 16, HALF), bf),
            pltpu.VMEM((NC, NCHIP, 16, HALF), bf),
            pltpu.VMEM((NCHIP, 16, HALF), bf),
            pltpu.VMEM((NCHIP, 16, HALF), bf),
            pltpu.VMEM((NCHIP, 16, HALF), f32),
            pltpu.VMEM((NCHIP, 16, HALF), bf),
            pltpu.VMEM((NCHIP, 16, HALF), bf),
            pltpu.VMEM((HEAD, 128), f32),
            pltpu.VMEM((8, 128), f32),
            pltpu.VMEM((HEAD, 128), f32),
            pltpu.VMEM((8, 128), f32),
            dma((2, 9)), dma((2, 9)),
            dma((2, 9, 4)), dma((2, 9, 4)),
            dma((4, 2)), dma((4, 2)),
            dma((2, 9)), dma((2, 9)),
            dma((8,)), dma((8,)),
            dma((NCHIP,)), dma((NCHIP,)),
            dma((NCHIP,)), dma((NCHIP,)),
            dma((NY,)), dma((NY,)),
            dma((NCHIP,)), dma((NCHIP,)),
        ],
        compiler_params=pltpu.CompilerParams(
            collective_id=0, has_side_effects=True
        ),
        name="layer",
    )(
        tokens.reshape(ROWS, D),
        queries.reshape(ROWS, 128),
        key_values.reshape(ROWS, 128),
        stop_bias.reshape(ROWS, 2).T,
        out_proj,
        norm_gain.reshape(1, D),
        up_proj,
        down_proj.T,
    )
    return out.reshape(8, 1, D)


def solution(mesh):
    return jax.shard_map(
        body,
        mesh=mesh,
        in_specs=(
            P("sp", None, None),
            P("sp", None, "tp"),
            P("sp", None, "tp"),
            P("sp", None, "tp"),
            P("tp", None),
            P(),
            P("sp", "tp"),
            P("tp", "sp"),
        ),
        out_specs=P(("sp", "tp"), None, None),
        check_vma=False,
    )
```

time: 77.5 us -> 68.3 us (0.88)
  Pallas kernels: 72.4 us -> 66.8 us
  local copies, waits for them, and re-layouts: 4.78 us -> 1.38 us
    pallas_call x1, Pallas kernels: 72.4 us -> 66.8 us  [body(): pl.pallas_call(kernel, out_shape=jax.ShapeDtypeStruct((8, D), bf), in_spe...]
    unnamed x17 -> x1, local copies, waits for them, and re-layouts: 4.78 us -> 1.38 us
where the time goes in v2:
time: 68.3 us; the launch traced here: 68.1 us
  Pallas kernels  66.8 us (98%)
  local copies, waits for them, and re-layouts  1.38 us (2%)
    pallas_call x1, Pallas kernels, body(): pl.pallas_call(kernel, out_shape=jax.ShapeDtypeStruct((8, D), bf), in_spe...  66.8 us
    unnamed x1, local copies, waits for them, and re-layouts  1.38 us

profile of v2, /device:TPU:1, one launch (start us, length us, event | category | flops | bytes accessed | tf_op | source)
XLA Modules:
  0.0 68.1 jit_solution(18009688205123931286)
XLA Ops:
  0.0 66.8 %layer.1 = bf16[8,2048]{1,0:T(8,128)(2,1)} custom-call(bf16[64,2048]{1,0:T(8,128)(2,1)} %bitcast.9, bf16[64,128]{1,0:T(8,128)(2,1)} %bitcast.12, bf16[64,128]{1,0:T(8,128)(2,1)} %bitcast.13, bf16[2,64]{1,0:T(2,128)(2,1)} %bitcast.15, bf16[128,2048]{1,0:T(8,128)(2,1)} %wo_hbm.1, f32[1,2048]{1,0:T(1,128)} %bitcast.14, bf16[32,512]{1,0:T(8,128)(2,1)} %up_hbm.1, ...), custom_call_target="tpu_custom_call" | custom-call | tf_op jit(solution)/shard_map/layer/pallas_call | solution.py:450
  66.8 1.4 %copy.10 = bf16[8,1,2048]{2,0,1:T(8,128)(2,1)} copy(bf16[8,1,2048]{2,0,1:T(8,128)(2,1)} %bitcast.10) | data formatting | bytes 65536

commit v3 on v2

--- a/solution.py
+++ b/solution.py
@@ -15,6 +15,8 @@
 EPSILON = 1e-06
 LOG2E = 1.4426950408889634
 UP_STEPS, DOWN_STEPS = 8, 7
+JUMP = 4
+W_PLAN = {0: ((1, 0),), 2: ((0, 0),), 3: ((1, 1),), 5: ((1, 2), (0, 1)), 6: ((0, 2),), 7: ((1, 3), (0, 3))}
 
 
 def nn(a, b):
@@ -33,7 +35,7 @@
     tok_hbm, q_hbm, kv_hbm, bias_hbm, wo_hbm, gain_hbm, up_hbm, down_hbm, out_ref,
     tok_ref, q_ref, bias_ref, wo_ref, gain_ref, up_ref, down_ref, in_s,
     kvall, wbuf, wcat, pbuf, prec, xbuf, e1, e1r, own, e2, erec,
-    u_hi, s_hi, u_lo, s_lo,
+    u_hi, s_hi, u_lo,
     kv_s, kv_r, yf_s, yf_r, we_s, we_r, w_s, w_r, p_s, p_r, x_s, x_r, xd_s, xd_r, e1_s, e1_r, e_s, e_r,
 ):
     sp = lax.axis_index("sp")
@@ -53,7 +55,7 @@
         )
 
     barrier = pltpu.get_barrier_semaphore()
-    peers = [(((z + d) % NZ) * NY + y, tp) for d in (1, 2, NZ - 2, NZ - 1)] + [sibling]
+    peers = [(((z + d + NZ) % NZ) * NY + y, tp) for d in range(-JUMP, JUMP + 1) if d] + [sibling]
     peers += [chip_at(r, c) for r in range(1, NCHIP)]
     peers += [chip_at(r, 1 - c) for r in range(1, NX)]
     for peer in peers:
@@ -82,71 +84,92 @@
     bias = jnp.concatenate([bias, jnp.zeros((14, HEAD), jnp.float32)], axis=0)
     bias = jnp.concatenate([bias, jnp.zeros((16, HEAD), jnp.float32)], axis=1)
     kvall[z, y, ROWS : ROWS + 16, :] = bias.astype(jnp.bfloat16)
-    u_hi[...] = jnp.zeros_like(u_hi)
     u_lo[...] = jnp.zeros_like(u_lo)
-    s_hi[...] = jnp.zeros_like(s_hi)
-    s_lo[...] = jnp.zeros_like(s_lo)
 
     loads[0].wait()
     pl.semaphore_wait(barrier, len(peers))
 
-    def along(buffer, send, recv, direction, d):
-        odd = d % 2
-        held = d - 2 + odd
-        hop = 2 - odd
+    def along(slot_of, send, recv, direction, d, held):
+        hop = d - held
         if direction == 0:
             p, to = (z - held + NZ) % NZ, (z + hop) % NZ
         else:
             p, to = (z + held) % NZ, (z - hop + NZ) % NZ
-        slot = buffer(p)
+        slot = slot_of(p)
         return rdma(slot, slot, send.at[direction, d], recv.at[direction, d], (to * NY + y, tp))
 
+    def held_at(d):
+        return (d - 1) // JUMP * JUMP
+
     def kv_copy(direction, d):
-        return along(lambda p: kvall.at[p, y], kv_s, kv_r, direction, d)
-
-    def kv_hand(direction, k, p, d):
-        slot = kvall.at[p, y]
+        return along(lambda p: kvall.at[p, y], kv_s, kv_r, direction, d, held_at(d))
+
+    def used(direction, d):
+        return (z - d >= 0) if direction == 0 else (z + d >= NZ) & (d <= DOWN_STEPS)
+
+    def place(direction, d):
+        return (z - d + NZ) % NZ if direction == 0 else (z + d) % NZ
+
+    def kv_sends(direction, d):
+        held = held_at(d)
+        if direction == 0:
+            return (z - held >= 0) & (z + d - held < NZ)
+        if d % JUMP == 0:
+            return (z + held) % NZ < DOWN_STEPS
+        return (z - d + held + NZ) % NZ + d >= NZ
+
+    def kv_arrives(direction, d):
+        if direction == 1 and d % JUMP == 0:
+            return (z + d) % NZ < DOWN_STEPS
+        return used(direction, d)
+
+    def kv_steps(direction):
+        return range(1, (UP_STEPS, DOWN_STEPS)[direction] + 1)
+
+    def kv_start(direction, d):
+        @pl.when(kv_sends(direction, d))
+        def _():
+            kv_copy(direction, d).start()
+
+    def kv_hand(direction, k, p, d, source=None):
+        slot = kvall.at[p, y if source is None else source]
         return rdma(
             slot, slot, yf_s.at[direction, k, d], yf_r.at[direction, k, d], (z * NY + (y + d) % NY, tp)
         )
 
-    def used(direction, d):
-        return (z - d >= 0) if direction == 0 else (z + d >= NZ) & (d <= DOWN_STEPS)
-
-    def place(direction, d):
-        return (z - d + NZ) % NZ if direction == 0 else (z + d) % NZ
-
-    def even_sends(direction, d):
-        if direction == 0:
-            return (d <= UP_STEPS) & (z - d + 2 >= 0) & (z + 2 < NZ)
-        return (d <= DOWN_STEPS) & ((z + d - 2) % NZ < DOWN_STEPS)
-
-    def even_arrives(direction, d):
-        if direction == 0:
-            return (d <= UP_STEPS) & (z - d >= 0)
-        return (d <= DOWN_STEPS) & ((z + d) % NZ < DOWN_STEPS)
-
-    def odd_sends(direction, d):
-        if direction == 0:
-            return (d <= UP_STEPS) & (z - d + 1 >= 0) & (z + 1 < NZ)
-        return (d <= DOWN_STEPS) & ((z + NZ - 1) % NZ + d >= NZ)
-
-    def odd_arrives(direction, d):
-        return (d <= UP_STEPS) & used(direction, d)
-
-    def kv_stage_sends(direction, j):
-        @pl.when(even_sends(direction, 2 * j))
+    def hand_start(direction, k, p):
+        kv_hand(direction, k, p, 1).start()
+        kv_hand(direction, k, p, 3).start()
+
+        @pl.when(c == 0)
         def _():
-            kv_copy(direction, 2 * j).start()
-
-        @pl.when(odd_sends(direction, 2 * j - 1))
+            kv_hand(direction, k, p, 2).start()
+
+    def relay(direction, k, p):
+        return rdma(
+            kvall.at[p, (y + 1) % NY], kvall.at[p, (y + 1) % NY],
+            yf_s.at[direction, k, 2], yf_r.at[direction, k, 2], (z * NY + (y + 3) % NY, tp),
+        )
+
+    def hand_relay(direction, k, p):
+        @pl.when(c == 1)
         def _():
-            kv_copy(direction, 2 * j - 1).start()
-
-    kv_stage_sends(0, 1)
-    kv_stage_sends(1, 1)
-    for d in range(1, NY):
-        kv_hand(0, 0, z, d).start()
+            kv_hand(direction, k, p, 3).wait_recv()
+            relay(direction, k, p).start()
+
+    def hand_wait(direction, k, p):
+        kv_hand(direction, k, p, 1).wait_recv()
+
+        @pl.when(c == 0)
+        def _():
+            kv_hand(direction, k, p, 3).wait_recv()
+
+        kv_hand(direction, k, p, 2).wait_recv()
+
+    for d in range(JUMP, 0, -1):
+        kv_start(0, d)
+        kv_start(1, d)
+    hand_start(0, 0, z)
 
     def w_hand(d, which):
         src = (up_ref, down_ref)[which]
@@ -169,7 +192,7 @@
         ]
 
     def w_copy(direction, d):
-        return along(lambda p: wbuf.at[p], w_s, w_r, direction, d)
+        return along(lambda p: wbuf.at[p], w_s, w_r, direction, d, (d - 1) // 2 * 2)
 
     def w_far(j):
         for direction, last in ((0, UP_STEPS), (1, DOWN_STEPS)):
@@ -188,6 +211,10 @@
         for direction, last in ((0, UP_STEPS), (1, DOWN_STEPS)):
             if 2 * j + 1 <= last:
                 w_copy(direction, 2 * j + 1).start()
+
+    def w_work(point):
+        for far, n in W_PLAN.get(point, ()):
+            (w_far if far else w_near)(n)
 
     def w_rest():
         for d in range(1, UP_STEPS, 2):
@@ -229,74 +256,83 @@
         values = jnp.concatenate([kvall[p, b, 0:ROWS, HEAD:128] for b in range(NY)], axis=0)
         return tn(values, weights), total
 
-    def attend_high(p, diagonal):
+    def attend_diagonal():
+        part, total = attend(z, True, 0.0)
+        u_hi[...] = part
+        s_hi[0:1, :] = total
+
+    def attend_high(d):
         carry = s_hi[0:1, :]
-        part, total = attend(p, diagonal, carry)
+        part, total = attend(place(0, d), False, carry)
         u_hi[...] += part
         s_hi[0:1, :] = carry + total
 
-    def attend_low(p):
-        part, total = attend(p, False, 0.0)
-        u_lo[...] = u_lo[...] * jnp.exp2(total) + part
-        s_lo[0:1, :] += total
-
-    def step(j, unused):
+    def attend_both(d):
+        carry = s_hi[0:1, :]
+        part, total = attend(place(0, d), False, carry)
+        part_low, total_low = attend(place(1, d), False, 0.0)
+        u_hi[...] += part
+        s_hi[0:1, :] = carry + total
+        u_lo[...] = u_lo[...] * jnp.exp2(total_low) + part_low
+
+    def kv_receive(d):
         for direction in range(2):
-            @pl.when(even_arrives(direction, 2 * j))
+            if d in kv_steps(direction):
+                @pl.when(kv_arrives(direction, d))
+                def _():
+                    kv_copy(direction, d).wait_recv()
+
+                if d % JUMP == 0:
+                    for further in range(d + JUMP, d, -1):
+                        if further in kv_steps(direction):
+                            kv_start(direction, further)
+
+                @pl.when(used(direction, d))
+                def _():
+                    hand_start(direction, d, place(direction, d))
+
+    def relay_step(d, unused):
+        for direction in range(2):
+            @pl.when(used(direction, d))
             def _():
-                kv_copy(direction, 2 * j).wait_recv()
-
-            kv_stage_sends(direction, j + 1)
-
-            @pl.when((2 * j <= UP_STEPS) & used(direction, 2 * j))
+                hand_relay(direction, d, place(direction, d))
+
+        return unused
+
+    def attend_step(d, unused):
+        for direction in range(2):
+            @pl.when(used(direction, d))
             def _():
-                for d in range(1, NY):
-                    kv_hand(direction, 2 * j, place(direction, 2 * j), d).start()
-
-            @pl.when(odd_arrives(direction, 2 * j - 1))
-            def _():
-                kv_copy(direction, 2 * j - 1).wait_recv()
-                for d in range(1, NY):
-                    kv_hand(direction, 2 * j - 1, place(direction, 2 * j - 1), d).start()
-
-        @pl.when(j == 2)
+                hand_wait(direction, d, place(direction, d))
+
+        @pl.when(used(1, d))
         def _():
-            w_far(0)
-
-        @pl.when(j == 3)
+            attend_both(d)
+
+        @pl.when(used(0, d) & jnp.logical_not(used(1, d)))
         def _():
-            w_near(0)
-
-        @pl.when(j == 4)
-        def _():
-            w_far(1)
-
-        @pl.when(j == 1)
-        def _():
-            for d in range(1, NY):
-                kv_hand(0, 0, z, d).wait_recv()
-            attend_high(z, True)
-
-        for back in (3, 2):
-            k = 2 * j - back
-
-            @pl.when((k > 0) & used(0, k))
-            def _():
-                for d in range(1, NY):
-                    kv_hand(0, k, place(0, k), d).wait_recv()
-                attend_high(place(0, k), False)
-
-            @pl.when((k > 0) & used(1, k))
-            def _():
-                for d in range(1, NY):
-                    kv_hand(1, k, place(1, k), d).wait_recv()
-                attend_low(place(1, k))
+            attend_high(d)
 
         return unused
 
-    lax.fori_loop(1, UP_STEPS // 2 + 2, step, 0)
-    w_near(1)
-    w_far(2)
+    hand_relay(0, 0, z)
+    w_work(0)
+    for d in (1, 2, 3, 4):
+        kv_receive(d)
+    w_work(1)
+    hand_wait(0, 0, z)
+    attend_diagonal()
+    lax.fori_loop(1, 5, relay_step, 0)
+    w_work(2)
+    for d in (5, 6, 7, 8):
+        kv_receive(d)
+    w_work(3)
+    lax.fori_loop(1, 5, attend_step, 0)
+    w_work(4)
+    lax.fori_loop(5, 9, relay_step, 0)
+    w_work(5)
+    lax.fori_loop(5, 9, attend_step, 0)
+    w_work(6)
 
     for load in loads[5:]:
         load.wait()
@@ -314,9 +350,7 @@
 
     for r in range(1, 8):
         p_copy(r).start()
-    w_near(2)
-    w_far(3)
-    w_near(3)
+    w_work(7)
     projected = pbuf[tp].astype(jnp.float32)
     for r in range(1, 8):
         p_copy(r).wait_recv()
@@ -343,6 +377,12 @@
             if dy or dx:
                 x_copy(dy * NX + dx).start()
     x_pass(0).start()
+    w_work(8)
+    for dy in rows_order:
+        for dx in (1, 3, 2, 0):
+            if dy or dx:
+                x_copy(dy * NX + dx).wait_recv()
+                x_pass(dy * NX + dx).start()
     w_far(4)
     w_rest()
     for p in range(8):
@@ -361,26 +401,25 @@
         target = ((y + dy) % NY) * NX + (x + dx) % NX
         return rdma(e2.at[target], erec.at[r], e_s.at[r], e_r.at[r], chip_at(r, c))
 
-    def feed_forward(dy):
-        for dx in (1, 3, 2, 0):
-            if dy or dx:
-                x_copy(dy * NX + dx).wait_recv()
-                x_pass(dy * NX + dx).start()
-        for dx in range(NX):
-            x_pass(dy * NX + dx).wait_recv()
-        rows = row_of(dy)
-        both = jnp.concatenate([xbuf[1 - c, rows], xbuf[c, rows]], axis=0).reshape(2 * NX * 16, HALF)
-        both = nn(both, wcat[...]).reshape(2 * NX, 16, 256)
+    def feed_forward(pair):
+        for dy in pair:
+            for dx in range(NX):
+                x_pass(dy * NX + dx).wait_recv()
+        tokens = jnp.concatenate([xbuf[core, row_of(dy)] for dy in pair for core in (1 - c, c)], axis=0)
+        both = nn(tokens.reshape(4 * NX * 16, HALF), wcat[...]).reshape(4 * NX, 16, 256)
         h = both[:, :8, :128] + both[:, 8:, 128:]
-        h = jnp.maximum(h.reshape(2 * NX * 8, 128), 0.0)
+        h = jnp.maximum(h.reshape(4 * NX * 8, 128), 0.0)
         h = (h * h).astype(jnp.bfloat16)
         for p in range(8):
             w = jnp.concatenate([wbuf[p, 1], wbuf[p + 8, 1]], axis=0)
-            o = nt(h, w).reshape(2 * NX, 8, 256)
+            o = nt(h, w).reshape(4 * NX, 8, 256)
             o = jnp.concatenate([o[:, :, :128], o[:, :, 128:]], axis=1)
-            e1[rows, :, p * 128 : (p + 1) * 128] = o[:NX].astype(jnp.bfloat16)
-            own[rows, :, p * 128 : (p + 1) * 128] = o[NX:]
-        swap(dy).start()
+            for n, dy in enumerate(pair):
+                at = 2 * NX * n
+                e1[row_of(dy), :, p * 128 : (p + 1) * 128] = o[at : at + NX].astype(jnp.bfloat16)
+                own[row_of(dy), :, p * 128 : (p + 1) * 128] = o[at + NX : at + 2 * NX]
+        for dy in pair:
+            swap(dy).start()
 
     def send_back(dy):
         swap(dy).wait_recv()
@@ -391,11 +430,12 @@
             if r:
                 e_copy(r).start()
 
-    for n, dy in enumerate(rows_order):
-        feed_forward(dy)
-        if n:
-            send_back(rows_order[n - 1])
-    send_back(rows_order[-1])
+    feed_forward(rows_order[:2])
+    send_back(rows_order[0])
+    send_back(rows_order[1])
+    feed_forward(rows_order[2:])
+    send_back(rows_order[2])
+    send_back(rows_order[3])
     update = own[chip] + e1r[chip].astype(jnp.float32)
     for dy in rows_order:
         for dx in range(NX):
@@ -406,25 +446,22 @@
     update = jnp.concatenate([update[:8], update[8:]], axis=1)
     out_ref[...] = (residual + update).astype(jnp.bfloat16)
 
-    def drain(j, unused):
+    for direction in range(2):
+        for d in kv_steps(direction):
+            @pl.when(kv_sends(direction, d))
+            def _():
+                kv_copy(direction, d).wait_send()
+
+    def drain(k, unused):
         for direction in range(2):
-            @pl.when(even_sends(direction, 2 * j))
+            @pl.when(used(direction, k))
             def _():
-                kv_copy(direction, 2 * j).wait_send()
-
-            @pl.when(odd_sends(direction, 2 * j - 1))
-            def _():
-                kv_copy(direction, 2 * j - 1).wait_send()
-
-            for k in (2 * j - 1, 2 * j):
-                @pl.when(used(direction, k))
-                def _():
-                    for d in range(1, NY):
-                        kv_hand(direction, k, place(direction, k), d).wait_send()
+                for d in range(1, NY):
+                    kv_hand(direction, k, place(direction, k), d).wait_send()
 
         return unused
 
-    lax.fori_loop(1, UP_STEPS // 2 + 1, drain, 0)
+    lax.fori_loop(1, UP_STEPS + 1, drain, 0)
     for d in range(1, NY):
         kv_hand(0, 0, z, d).wait_send()
         for which in range(2):
@@ -475,7 +512,6 @@
             pltpu.VMEM((HEAD, 128), f32),
             pltpu.VMEM((8, 128), f32),
             pltpu.VMEM((HEAD, 128), f32),
-            pltpu.VMEM((8, 128), f32),
             dma((2, 9)), dma((2, 9)),
             dma((2, 9, 4)), dma((2, 9, 4)),
             dma((4, 2)), dma((4, 2)),

time: 68.3 us -> 64.5 us (0.944)
  Pallas kernels: 66.8 us -> 62.9 us
    pallas_call x1, Pallas kernels: 66.8 us -> 62.9 us  [body(): pl.pallas_call(kernel, out_shape=jax.ShapeDtypeStruct((8, D), bf), in_spe...]
where the time goes in v3:
time: 64.5 us; the launch traced here: 64.3 us
  Pallas kernels  62.9 us (98%)
  local copies, waits for them, and re-layouts  1.38 us (2%)
    pallas_call x1, Pallas kernels, body(): pl.pallas_call(kernel, out_shape=jax.ShapeDtypeStruct((8, D), bf), in_spe...  62.9 us
    unnamed x1, local copies, waits for them, and re-layouts  1.38 us

profile of v3, /device:TPU:1, one launch (start us, length us, event | category | flops | bytes accessed | tf_op | source)
XLA Modules:
  0.0 64.3 jit_solution(8271218382131256463)
XLA Ops:
  0.0 62.9 %layer.1 = bf16[8,2048]{1,0:T(8,128)(2,1)} custom-call(bf16[64,2048]{1,0:T(8,128)(2,1)} %bitcast.9, bf16[64,128]{1,0:T(8,128)(2,1)} %bitcast.12, bf16[64,128]{1,0:T(8,128)(2,1)} %bitcast.13, bf16[2,64]{1,0:T(2,128)(2,1)} %bitcast.15, bf16[128,2048]{1,0:T(8,128)(2,1)} %wo_hbm.1, f32[1,2048]{1,0:T(1,128)} %bitcast.14, bf16[32,512]{1,0:T(8,128)(2,1)} %up_hbm.1, ...), custom_call_target="tpu_custom_call" | custom-call | tf_op jit(solution)/shard_map/layer/pallas_call | solution.py:487
  63.0 1.4 %copy.10 = bf16[8,1,2048]{2,0,1:T(8,128)(2,1)} copy(bf16[8,1,2048]{2,0,1:T(8,128)(2,1)} %bitcast.10) | data formatting | bytes 65536

commit v4 on v3

--- a/solution.py
+++ b/solution.py
@@ -16,7 +16,7 @@
 LOG2E = 1.4426950408889634
 UP_STEPS, DOWN_STEPS = 8, 7
 JUMP = 4
-W_PLAN = {0: ((1, 0),), 2: ((0, 0),), 3: ((1, 1),), 5: ((1, 2), (0, 1)), 6: ((0, 2),), 7: ((1, 3), (0, 3))}
+W_PLAN = {0: ((1, 0),), 1: ((0, 0),), 2: ((1, 1),), 3: ((0, 1),), 5: ((1, 2),), 6: ((0, 2),), 7: ((1, 3), (0, 3))}
 
 
 def nn(a, b):
@@ -194,11 +194,12 @@
     def w_copy(direction, d):
         return along(lambda p: wbuf.at[p], w_s, w_r, direction, d, (d - 1) // 2 * 2)
 
-    def w_far(j):
-        for direction, last in ((0, UP_STEPS), (1, DOWN_STEPS)):
+    def w_far(j, ways=(0, 1)):
+        for direction in ways:
+            last = (UP_STEPS, DOWN_STEPS)[direction]
             if 2 * j <= last:
                 if j == 0:
-                    if direction == 0:
+                    if direction == ways[0]:
                         for d in range(1, NY):
                             for which in range(2):
                                 w_hand(d, which).wait_recv()
@@ -207,14 +208,15 @@
             if 2 * j + 2 <= last:
                 w_copy(direction, 2 * j + 2).start()
 
-    def w_near(j):
-        for direction, last in ((0, UP_STEPS), (1, DOWN_STEPS)):
+    def w_near(j, ways=(0, 1)):
+        for direction in ways:
+            last = (UP_STEPS, DOWN_STEPS)[direction]
             if 2 * j + 1 <= last:
                 w_copy(direction, 2 * j + 1).start()
 
     def w_work(point):
-        for far, n in W_PLAN.get(point, ()):
-            (w_far if far else w_near)(n)
+        for far, *step in W_PLAN.get(point, ()):
+            (w_far if far else w_near)(*step)
 
     def w_rest():
         for d in range(1, UP_STEPS, 2):

time: 64.5 us -> 62.2 us (0.964)
  Pallas kernels: 62.9 us -> 60.6 us
    pallas_call x1, Pallas kernels: 62.9 us -> 60.6 us  [body(): pl.pallas_call(kernel, out_shape=jax.ShapeDtypeStruct((8, D), bf), in_spe...]
where the time goes in v4:
time: 62.2 us; the launch traced here: 62 us
  Pallas kernels  60.6 us (97%)
  local copies, waits for them, and re-layouts  1.38 us (2%)
    pallas_call x1, Pallas kernels, body(): pl.pallas_call(kernel, out_shape=jax.ShapeDtypeStruct((8, D), bf), in_spe...  60.6 us
    unnamed x1, local copies, waits for them, and re-layouts  1.38 us

profile of v4, /device:TPU:1, one launch (start us, length us, event | category | flops | bytes accessed | tf_op | source)
XLA Modules:
  0.0 62.0 jit_solution(4231351641907995474)
XLA Ops:
  0.0 60.6 %layer.1 = bf16[8,2048]{1,0:T(8,128)(2,1)} custom-call(bf16[64,2048]{1,0:T(8,128)(2,1)} %bitcast.9, bf16[64,128]{1,0:T(8,128)(2,1)} %bitcast.12, bf16[64,128]{1,0:T(8,128)(2,1)} %bitcast.13, bf16[2,64]{1,0:T(2,128)(2,1)} %bitcast.15, bf16[128,2048]{1,0:T(8,128)(2,1)} %wo_hbm.1, f32[1,2048]{1,0:T(1,128)} %bitcast.14, bf16[32,512]{1,0:T(8,128)(2,1)} %up_hbm.1, ...), custom_call_target="tpu_custom_call" | custom-call | tf_op jit(solution)/shard_map/layer/pallas_call | solution.py:489
  60.6 1.4 %copy.10 = bf16[8,1,2048]{2,0,1:T(8,128)(2,1)} copy(bf16[8,1,2048]{2,0,1:T(8,128)(2,1)} %bitcast.10) | data formatting | bytes 65536

commit v5 on v4

--- a/solution.py
+++ b/solution.py
@@ -81,9 +81,9 @@
 
     loads[1].wait()
     bias = bias_ref[...].astype(jnp.float32)
-    bias = jnp.concatenate([bias, jnp.zeros((14, HEAD), jnp.float32)], axis=0)
-    bias = jnp.concatenate([bias, jnp.zeros((16, HEAD), jnp.float32)], axis=1)
-    kvall[z, y, ROWS : ROWS + 16, :] = bias.astype(jnp.bfloat16)
+    bias = jnp.concatenate([bias, jnp.zeros((6, HEAD), jnp.float32)], axis=0)
+    bias = jnp.concatenate([bias, jnp.zeros((8, HEAD), jnp.float32)], axis=1)
+    kvall[z, y, ROWS : ROWS + 8, :] = bias.astype(jnp.bfloat16)
     u_lo[...] = jnp.zeros_like(u_lo)
 
     loads[0].wait()
@@ -141,28 +141,12 @@
         kv_hand(direction, k, p, 1).start()
         kv_hand(direction, k, p, 3).start()
 
-        @pl.when(c == 0)
-        def _():
-            kv_hand(direction, k, p, 2).start()
-
-    def relay(direction, k, p):
-        return rdma(
-            kvall.at[p, (y + 1) % NY], kvall.at[p, (y + 1) % NY],
-            yf_s.at[direction, k, 2], yf_r.at[direction, k, 2], (z * NY + (y + 3) % NY, tp),
-        )
-
-    def hand_relay(direction, k, p):
-        @pl.when(c == 1)
-        def _():
-            kv_hand(direction, k, p, 3).wait_recv()
-            relay(direction, k, p).start()
+        kv_hand(direction, k, p, 2).start()
 
     def hand_wait(direction, k, p):
         kv_hand(direction, k, p, 1).wait_recv()
 
-        @pl.when(c == 0)
-        def _():
-            kv_hand(direction, k, p, 3).wait_recv()
+        kv_hand(direction, k, p, 3).wait_recv()
 
         kv_hand(direction, k, p, 2).wait_recv()
 
@@ -226,8 +210,8 @@
     loads[4].wait()
     q = q_ref[...].astype(jnp.float32) * 0.125
     queries = jnp.concatenate([q[:, :HEAD], q[:, HEAD:]], axis=0).astype(jnp.bfloat16)
-    pick = lax.broadcasted_iota(jnp.int32, (16, 128), 1) // HEAD
-    pick = (pick == lax.broadcasted_iota(jnp.int32, (16, 128), 0)).astype(jnp.float32).astype(jnp.bfloat16)
+    pick = lax.broadcasted_iota(jnp.int32, (8, 128), 1) // HEAD
+    pick = (pick == lax.broadcasted_iota(jnp.int32, (8, 128), 0)).astype(jnp.float32).astype(jnp.bfloat16)
     later = lax.broadcasted_iota(jnp.int32, (256, 256), 1) > lax.broadcasted_iota(jnp.int32, (256, 256), 0)
     later = later.astype(jnp.float32).astype(jnp.bfloat16)
 
@@ -235,7 +219,7 @@
         parts = []
         for b in range(NY):
             keys = kvall[p, b, 0:ROWS, 0:HEAD]
-            biases = kvall[p, b, ROWS : ROWS + 16, 0:HEAD]
+            biases = kvall[p, b, ROWS : ROWS + 8, 0:HEAD]
             parts.append(nt(keys, queries) + tn(biases, pick))
         score = jnp.concatenate(parts, axis=0) * LOG2E
         tail = jnp.log2(1.0 + jnp.exp2(-jnp.abs(score)))
@@ -293,14 +277,6 @@
                 def _():
                     hand_start(direction, d, place(direction, d))
 
-    def relay_step(d, unused):
-        for direction in range(2):
-            @pl.when(used(direction, d))
-            def _():
-                hand_relay(direction, d, place(direction, d))
-
-        return unused
-
     def attend_step(d, unused):
         for direction in range(2):
             @pl.when(used(direction, d))
@@ -317,21 +293,19 @@
 
         return unused
 
-    hand_relay(0, 0, z)
     w_work(0)
     for d in (1, 2, 3, 4):
         kv_receive(d)
     w_work(1)
     hand_wait(0, 0, z)
     attend_diagonal()
-    lax.fori_loop(1, 5, relay_step, 0)
     w_work(2)
+    lax.fori_loop(1, 3, attend_step, 0)
     for d in (5, 6, 7, 8):
         kv_receive(d)
     w_work(3)
-    lax.fori_loop(1, 5, attend_step, 0)
+    lax.fori_loop(3, 5, attend_step, 0)
     w_work(4)
-    lax.fori_loop(5, 9, relay_step, 0)
     w_work(5)
     lax.fori_loop(5, 9, attend_step, 0)
     w_work(6)
@@ -500,7 +474,7 @@
             pltpu.VMEM((32, 512), bf),
             pltpu.VMEM((32, 512), bf),
             dma((8,)),
-            pltpu.VMEM((NZ, NY, ROWS + 16, 128), bf),
+            pltpu.VMEM((NZ, NY, ROWS + 8, 128), bf),
             pltpu.VMEM((NZ, 2, 128, 128), bf),
             pltpu.VMEM((HALF, 256), bf),
             pltpu.VMEM((8, 16, HALF), bf),

time: 62.2 us -> 60.7 us (0.976)
  Pallas kernels: 60.6 us -> 59.1 us
    pallas_call x1, Pallas kernels: 60.6 us -> 59.1 us  [body(): pl.pallas_call(kernel, out_shape=jax.ShapeDtypeStruct((8, D), bf), in_spe...]
where the time goes in v5:
time: 60.7 us; the launch traced here: 60.5 us
  Pallas kernels  59.1 us (97%)
  local copies, waits for them, and re-layouts  1.38 us (2%)
    pallas_call x1, Pallas kernels, body(): pl.pallas_call(kernel, out_shape=jax.ShapeDtypeStruct((8, D), bf), in_spe...  59.1 us
    unnamed x1, local copies, waits for them, and re-layouts  1.38 us

profile of v5, /device:TPU:1, one launch (start us, length us, event | category | flops | bytes accessed | tf_op | source)
XLA Modules:
  0.0 60.5 jit_solution(1172431389471154987)
XLA Ops:
  0.0 59.1 %layer.1 = bf16[8,2048]{1,0:T(8,128)(2,1)} custom-call(bf16[64,2048]{1,0:T(8,128)(2,1)} %bitcast.9, bf16[64,128]{1,0:T(8,128)(2,1)} %bitcast.12, bf16[64,128]{1,0:T(8,128)(2,1)} %bitcast.13, bf16[2,64]{1,0:T(2,128)(2,1)} %bitcast.15, bf16[128,2048]{1,0:T(8,128)(2,1)} %wo_hbm.1, f32[1,2048]{1,0:T(1,128)} %bitcast.14, bf16[32,512]{1,0:T(8,128)(2,1)} %up_hbm.1, ...), custom_call_target="tpu_custom_call" | custom-call | tf_op jit(solution)/shard_map/layer/pallas_call | solution.py:463
  59.2 1.4 %copy.10 = bf16[8,1,2048]{2,0,1:T(8,128)(2,1)} copy(bf16[8,1,2048]{2,0,1:T(8,128)(2,1)} %bitcast.10) | data formatting | bytes 65536

commit v6 on v5

--- a/solution.py
+++ b/solution.py
@@ -324,11 +324,11 @@
         to = (tp + r) % 8
         return rdma(pbuf.at[to], prec.at[r], p_s.at[r], p_r.at[r], (sp, to))
 
-    for r in range(1, 8):
+    for r in (4, 5, 3, 2, 6, 7, 1):
         p_copy(r).start()
     w_work(7)
     projected = pbuf[tp].astype(jnp.float32)
-    for r in range(1, 8):
+    for r in (1, 7, 6, 2, 3, 5, 4):
         p_copy(r).wait_recv()
         projected = projected + prec[r].astype(jnp.float32)
     projected = jnp.concatenate([projected[:8], projected[8:]], axis=1)

time: 60.7 us -> 60.7 us (level)
  no operation moved by 1% of the time
where the time goes in v6:
time: 60.7 us; the launch traced here: 60.5 us
  Pallas kernels  59.1 us (97%)
  local copies, waits for them, and re-layouts  1.38 us (2%)
    pallas_call x1, Pallas kernels, body(): pl.pallas_call(kernel, out_shape=jax.ShapeDtypeStruct((8, D), bf), in_spe...  59.1 us
    unnamed x1, local copies, waits for them, and re-layouts  1.38 us

profile of v6, /device:TPU:1, one launch (start us, length us, event | category | flops | bytes accessed | tf_op | source)
XLA Modules:
  0.0 60.5 jit_solution(2491651482630192935)
XLA Ops:
  0.0 59.1 %layer.1 = bf16[8,2048]{1,0:T(8,128)(2,1)} custom-call(bf16[64,2048]{1,0:T(8,128)(2,1)} %bitcast.9, bf16[64,128]{1,0:T(8,128)(2,1)} %bitcast.12, bf16[64,128]{1,0:T(8,128)(2,1)} %bitcast.13, bf16[2,64]{1,0:T(2,128)(2,1)} %bitcast.15, bf16[128,2048]{1,0:T(8,128)(2,1)} %wo_hbm.1, f32[1,2048]{1,0:T(1,128)} %bitcast.14, bf16[32,512]{1,0:T(8,128)(2,1)} %up_hbm.1, ...), custom_call_target="tpu_custom_call" | custom-call | tf_op jit(solution)/shard_map/layer/pallas_call | solution.py:463
  59.1 1.4 %copy.10 = bf16[8,1,2048]{2,0,1:T(8,128)(2,1)} copy(bf16[8,1,2048]{2,0,1:T(8,128)(2,1)} %bitcast.10) | data formatting | bytes 65536

commit v7 on v6

--- a/solution.py
+++ b/solution.py
@@ -16,7 +16,7 @@
 LOG2E = 1.4426950408889634
 UP_STEPS, DOWN_STEPS = 8, 7
 JUMP = 4
-W_PLAN = {0: ((1, 0),), 1: ((0, 0),), 2: ((1, 1),), 3: ((0, 1),), 5: ((1, 2),), 6: ((0, 2),), 7: ((1, 3), (0, 3))}
+W_PLAN = {0: ((1, 0),), 1: ((0, 0),), 2: ((1, 1),), 3: ((0, 1),), 5: ((1, 2), (0, 2)), 7: ((1, 3), (0, 3))}
 
 
 def nn(a, b):
@@ -408,8 +408,8 @@
 
     feed_forward(rows_order[:2])
     send_back(rows_order[0])
+    feed_forward(rows_order[2:])
     send_back(rows_order[1])
-    feed_forward(rows_order[2:])
     send_back(rows_order[2])
     send_back(rows_order[3])
     update = own[chip] + e1r[chip].astype(jnp.float32)

time: 60.7 us -> 60.6 us (level)
  no operation moved by 1% of the time
where the time goes in v7:
time: 60.6 us; the launch traced here: 60.5 us
  Pallas kernels  59.1 us (98%)
  local copies, waits for them, and re-layouts  1.38 us (2%)
    pallas_call x1, Pallas kernels, body(): pl.pallas_call(kernel, out_shape=jax.ShapeDtypeStruct((8, D), bf), in_spe...  59.1 us
    unnamed x1, local copies, waits for them, and re-layouts  1.38 us

profile of v7, /device:TPU:1, one launch (start us, length us, event | category | flops | bytes accessed | tf_op | source)
XLA Modules:
  0.0 60.5 jit_solution(6047648666615319300)
XLA Ops:
  0.0 59.1 %layer.1 = bf16[8,2048]{1,0:T(8,128)(2,1)} custom-call(bf16[64,2048]{1,0:T(8,128)(2,1)} %bitcast.9, bf16[64,128]{1,0:T(8,128)(2,1)} %bitcast.12, bf16[64,128]{1,0:T(8,128)(2,1)} %bitcast.13, bf16[2,64]{1,0:T(2,128)(2,1)} %bitcast.15, bf16[128,2048]{1,0:T(8,128)(2,1)} %wo_hbm.1, f32[1,2048]{1,0:T(1,128)} %bitcast.14, bf16[32,512]{1,0:T(8,128)(2,1)} %up_hbm.1, ...), custom_call_target="tpu_custom_call" | custom-call | tf_op jit(solution)/shard_map/layer/pallas_call | solution.py:463
  59.1 1.4 %copy.10 = bf16[8,1,2048]{2,0,1:T(8,128)(2,1)} copy(bf16[8,1,2048]{2,0,1:T(8,128)(2,1)} %bitcast.10) | data formatting | bytes 65536
